TPU v7x, 32 devices: a whole 2x2x4 slice. The times are simulated.
32 devices in a mesh: sp: 8 (over z, x), tp: 4 (over y, core).
Axes of the slice: x: 2, y: 2, z: 4, core: 2. Of those that a mesh axis runs over, the one named last changes fastest.
Arguments:
- queries: bfloat16 [1024, 2048], P('sp', 'tp'), may hold values from -18 to 90
- projected_key_rows: bfloat16 [1024, 1024], P('sp', 'tp'), may hold values from -18 to 90
- projected_value_rows: bfloat16 [1024, 1024], P('sp', 'tp'), may hold values from -6 to 6
- query_gain: float32 [64], replicated, may hold values from 1 to 6
- key_norm_gain: float32 [64], replicated, may hold values from 1 to 6
- residual: bfloat16 [1024, 2048], P('sp', 'tp'), may hold values from -54 to 54
- out_weight: bfloat16 [2048, 2048], P('tp'), may hold values from -1 to 1
- norm_gain: float32 [2048], P('tp'), may hold values from 0.28 to 4.68
- expert_ids: int32 [1024, 2], P('sp'), may hold values from 0 to 7, as said below
- route_weights: float32 [1024, 2], P('sp'), may hold values from 0.2 to 1
- gate_weight: bfloat16 [8, 2048, 4096], P('sp', None, 'tp'), may hold values from -0.125 to 0.125
- up_weight: bfloat16 [8, 2048, 4096], P('sp', None, 'tp'), may hold values from -0.125 to 0.125
- down_weight: bfloat16 [8, 4096, 2048], P('sp', 'tp'), may hold values from -0.25 to 0.25
- final_gain: float32 [2048], P('tp'), may hold values from 0.1 to 1.9
Outputs:
- layer_out: bfloat16 [1024, 2048], P('sp', 'tp')
Inputs may be any that keep to these rules, and one draw needn't show every extreme that they name: `expert_ids`: each row names two different experts of one group, the group of expert e being e // 4. In every aligned block of 128 rows each group is named by the same number of rows, no expert is named by more than 64 rows, one expert of every group is named by exactly 64 rows, and one expert is named by 64 rows of every block.
All inputs are finite; a program needn't handle non-finite values.
Results may differ from a plain program's by a relative error of at most 0.019.
The roundings to bfloat16 on the way count: a program that leaves them out, or rounds other values in their place, can miss the bound.
Values may be sent and summed in bfloat16 or wider, within the bound.
A program may use at most 64 MiB of HBM per device.

v0:
```python
import jax
import jax.numpy as jnp
from jax import lax
from jax.experimental import pallas as pl
from jax.experimental.pallas import tpu as pltpu
from jax.sharding import PartitionSpec as P

D = 2048
HEAD_DIM = 64
GRID_W = 64
TOPK = 2


theta_base = 10000.0
norm_epsilon = 1e-06
residual_scale = 8.0**0.25
far_below = -1e30
MESH = pl.DeviceIdType.MESH


def rope_line(halves, angles):
    pair_count = angles.shape[-1]
    first_half = halves[..., :pair_count]
    second_half = halves[..., pair_count:]
    cosine = jnp.cos(angles)[:, None, :]
    sine_part = jnp.sin(angles)[:, None, :]
    return jnp.concatenate(
        [
            first_half * cosine - second_half * sine_part,
            first_half * sine_part + second_half * cosine,
        ],
        -1,
    )


def rotary_over_grid(rows_by_head, token_positions):
    head_size = rows_by_head.shape[-1]
    frequency = theta_base ** (
        -jnp.arange(0, head_size // 2, 2, dtype=jnp.float32) / (head_size // 2)
    )
    grid_row = (token_positions // GRID_W).astype(jnp.float32)
    grid_col = (token_positions % GRID_W).astype(jnp.float32)
    row_part = rope_line(
        rows_by_head[..., : head_size // 2], grid_row[:, None] * frequency[None, :]
    )
    col_part = rope_line(
        rows_by_head[..., head_size // 2 :], grid_col[:, None] * frequency[None, :]
    )
    return jnp.concatenate([row_part, col_part], -1)


def normalize_heads(token_rows, gain_row, head_count):
    shaped = token_rows.astype(jnp.float32).reshape(token_rows.shape[0], head_count, -1)
    scaled = shaped * lax.rsqrt(jnp.mean(shaped * shaped, -1, keepdims=True) + norm_epsilon)
    return scaled * gain_row[None, None, :]


def ring_gather(packed, group, group_minor):
    rows, width = packed.shape
    pieces = 4
    piece = rows // pieces
    half = group // 2
    major = group // group_minor

    def place_of(index):
        high, low = index // group_minor, lax.rem(index, group_minor)
        if group_minor == 1:
            return high
        back = major - 1 - high
        odd = lax.rem(back, 2)
        inner = (low - 1) * (1 - odd) + (group_minor - 1 - low) * odd
        first = jnp.where(low == 0, 1, 0)
        return first * high + (1 - first) * (major + back * (group_minor - 1) + inner)

    def device_at(place):
        if group_minor == 1:
            return place
        first = jnp.where(place < major, 1, 0)
        rest = jnp.maximum(place - major, 0)
        back = rest // (group_minor - 1)
        inner = lax.rem(rest, group_minor - 1)
        odd = lax.rem(back, 2)
        low = 1 + inner * (1 - odd) + (group_minor - 2 - inner) * odd
        other = (major - 1 - back) * group_minor + low
        return first * (place * group_minor) + (1 - first) * other

    def kernel(mine_ref, all_ref, send_sem, recv_sem, own_sem):
        me = lax.axis_index("sp")
        spot = place_of(me)
        right = device_at(lax.rem(spot + 1, group))
        left = device_at(lax.rem(spot + group - 1, group))
        barrier = pltpu.get_barrier_semaphore()
        for neighbour in (left, right):
            pl.semaphore_signal(
                barrier, inc=1, device_id={"sp": neighbour}, device_id_type=MESH
            )
        pl.semaphore_wait(barrier, 2)
        own = pltpu.make_async_copy(mine_ref, all_ref.at[0], own_sem)
        own.start()
        copies = {}
        for hop in range(1, half + 1):
            for part in range(pieces):
                span = pl.ds(part * piece, piece)
                for way in range(2):
                    if hop == half and (part < pieces // 2) != (way == 0):
                        continue
                    if hop > 1:
                        copies[way, hop - 1, part].wait_recv()
                    source_slot = (hop - 1) if way == 0 else (group - hop + 1)
                    target_slot = hop if way == 0 else group - hop
                    source = mine_ref.at[span] if hop == 1 else all_ref.at[source_slot, span]
                    copy = pltpu.make_async_remote_copy(
                        src_ref=source,
                        dst_ref=all_ref.at[target_slot, span],
                        send_sem=send_sem.at[way, hop - 1, part],
                        recv_sem=recv_sem.at[way, hop - 1, part],
                        device_id={"sp": right if way == 0 else left},
                        device_id_type=MESH,
                    )
                    copy.start()
                    copies[way, hop, part] = copy
        for way, hop, part in copies:
            if hop == half or (hop == half - 1 and (way, half, part) not in copies):
                copies[way, hop, part].wait_recv()
        for copy in copies.values():
            copy.wait_send()
        own.wait()

    return pl.pallas_call(
        kernel,
        out_shape=jax.ShapeDtypeStruct((group, rows, width), packed.dtype),
        in_specs=[pl.BlockSpec(memory_space=pltpu.VMEM)],
        out_specs=pl.BlockSpec(memory_space=pltpu.VMEM),
        scratch_shapes=[
            pltpu.SemaphoreType.DMA((2, half, pieces)),
            pltpu.SemaphoreType.DMA((2, half, pieces)),
            pltpu.SemaphoreType.DMA,
        ],
        compiler_params=pltpu.CompilerParams(
            collective_id=0, has_side_effects=True, vmem_limit_bytes=24 << 20
        ),
    )(packed)


def after_attention(
    attended, out_weight, residual, norm_gain, places, route_weights, gate_weight, up_weight,
    down_weight, final_gain, experts, shards,
):
    token_count, width = residual.shape
    lines = shards // 2
    row_total = TOPK * 2 * token_count
    capacity = row_total // experts
    groups = 4
    group_rows = row_total // groups
    group_experts = experts // groups
    halves = groups
    half_rows = row_total // halves
    hidden_units = gate_weight.shape[2]
    tile = min(256, hidden_units)
    feature_total = width * shards
    places_across = places.T
    bf16, f32 = jnp.bfloat16, jnp.float32

    def kernel(
        att_ref, ow_ref, res_ref, gain_ref, at_ref, across_ref, rw_ref, gate_hbm, up_hbm, down_hbm,
        last_gain_ref, out_ref,
        gate_v, up_v, down_v, weight_sem,
        mix_send, mix_pair, line_send, line_recv, mix_sem, line_sem,
        stat_send, stat_recv, stat_sem,
        outgoing, routed, out_sem, fwd_sem, cross_sem, relay_sem,
        hidden, part_send, part_pair, sum_send, sum_recv, own_sum, other_sum, part_sem, sum_sem,
        result, returned, back_sem,
    ):
        me_s = lax.axis_index("sp")
        me_t = lax.axis_index("tp")
        line = me_t // 2
        core = lax.rem(me_t, 2)
        partner = line * 2 + 1 - core

        def line_at(step):
            return lax.rem(line + step, lines)

        barrier = pltpu.get_barrier_semaphore()
        for step in range(1, experts):
            pl.semaphore_signal(
                barrier, inc=1, device_id={"sp": lax.rem(me_s + step, experts)},
                device_id_type=MESH,
            )
        for step in range(1, shards):
            pl.semaphore_signal(
                barrier, inc=1, device_id={"tp": lax.rem(me_t + step, shards)},
                device_id_type=MESH,
            )
        loads = [
            pltpu.make_async_copy(src.at[0], dst, weight_sem.at[i])
            for i, (src, dst) in enumerate(
                ((gate_hbm, gate_v), (up_hbm, up_v), (down_hbm, down_v))
            )
        ]
        for load in loads:
            load.start()
        sent = []

        def push(source, target, sems, index, device):
            copy = pltpu.make_async_remote_copy(
                src_ref=source, dst_ref=target,
                send_sem=sems.at[(0,) + index], recv_sem=sems.at[(1,) + index],
                device_id=device, device_id_type=MESH,
            )
            copy.start()
            sent.append(copy)
            return copy

        attended_rows = att_ref[...]

        def mix(shard):
            return jnp.dot(
                attended_rows,
                ow_ref[:, pl.ds(pl.multiple_of(shard * width, width), width)],
                preferred_element_type=f32,
            )

        for step in range(lines):
            mix_send[step] = mix(line_at(step) * 2 + 1 - core).astype(bf16)
        pl.semaphore_wait(barrier, experts + shards - 2)
        pair = {}
        for step in list(range(1, lines)) + [0]:
            pair[step] = push(
                mix_send.at[step], mix_pair.at[step], mix_sem, (step,), {"tp": partner}
            )
        across = {}
        for step in range(1, lines):
            mine = mix(line_at(step) * 2 + core)
            pair[step].wait_recv()
            line_send[step - 1] = (mine + mix_pair[step].astype(f32)).astype(bf16)
            across[step] = push(
                line_send.at[step - 1], line_recv.at[step - 1], line_sem, (step - 1,),
                {"tp": line_at(step) * 2 + core},
            )
        total = mix(me_t)
        pair[0].wait_recv()
        total = total + mix_pair[0].astype(f32)
        total = total + residual_scale * res_ref[...].astype(f32)
        for step in range(1, lines):
            across[step].wait_recv()
            total = total + line_recv[step - 1].astype(f32)

        lane = lax.broadcasted_iota(jnp.int32, (token_count, 128), 1)

        def normalize(values, gain, turn):
            sums = jnp.sum(values, 1, keepdims=True)
            squares = jnp.sum(values * values, 1, keepdims=True)
            both = jnp.where(lane == 0, sums, jnp.where(lane == 1, squares, 0.0)).T[:8]
            stat_send[turn] = both
            stats = [
                push(
                    stat_send.at[turn], stat_recv.at[turn, step - 1], stat_sem,
                    (turn, step - 1), {"tp": lax.rem(me_t + step, shards)},
                )
                for step in range(1, shards)
            ]
            for step in range(1, shards):
                stats[step - 1].wait_recv()
                both = both + stat_recv[turn, step - 1]
            columns = jnp.concatenate([both] * 16, 0).T
            center = columns[:, 0:1] / feature_total
            spread = columns[:, 1:2] / feature_total - center * center
            return (values - center) * lax.rsqrt(spread + norm_epsilon) * gain

        normed = normalize(total, gain_ref[...], 0).astype(bf16)
        row_index = lax.broadcasted_iota(jnp.int32, (row_total, token_count), 0)
        picks = jnp.where(
            (row_index == across_ref[0:1, :]) | (row_index == across_ref[1:2, :]), 1.0, 0.0
        ).astype(bf16)
        spread_rows = jnp.dot(picks, normed, preferred_element_type=f32).astype(bf16)
        outgoing[...] = spread_rows
        routed[me_t, pl.ds(0, capacity)] = spread_rows[:capacity]
        arrivals = {}
        for step in range(1, experts):
            rows = pl.ds(step * capacity, capacity)
            arrivals[step] = push(
                outgoing.at[rows], routed.at[me_t, rows], out_sem, (step,),
                {"sp": lax.rem(me_s + step, experts)},
            )
        forwards, crossings, relays = {}, {}, {}

        def forward(group):
            for step in range(group * group_experts, (group + 1) * group_experts):
                if step > 0:
                    arrivals[step].wait_recv()
            rows = pl.ds(group * group_rows, group_rows)
            block = routed.at[me_t, rows]
            for step in range(1, lines):
                crossings[group, step] = push(
                    block, block, cross_sem, (group, step - 1),
                    {"tp": line_at(step) * 2 + core},
                )
            forwards[group] = push(block, block, fwd_sem, (group,), {"tp": partner})

        def relay(group):
            rows = pl.ds(group * group_rows, group_rows)
            for step in range(1, lines):
                crossings[group, step].wait_recv()
                block = routed.at[line_at(lines - step) * 2 + core, rows]
                relays[group, step] = push(
                    block, block, relay_sem, (group, step - 1), {"tp": partner}
                )

        def settle(group):
            forwards[group].wait_recv()
            for step in range(1, lines):
                relays[group, step].wait_recv()

        def expand(half):
            rows = pl.ds(half * half_rows, half_rows)

            def one_tile(index, carry):
                cols = pl.ds(pl.multiple_of(index * tile, tile), tile)
                gate_sum = jnp.zeros((half_rows, tile), f32)
                up_sum = jnp.zeros((half_rows, tile), f32)
                for shard in range(shards):
                    block = routed[shard, rows]
                    deep = pl.ds(shard * width, width)
                    gate_sum += jnp.dot(block, gate_v[deep, cols], preferred_element_type=f32)
                    up_sum += jnp.dot(block, up_v[deep, cols], preferred_element_type=f32)
                hidden[rows, cols] = (
                    gate_sum / (1.0 + jnp.exp(-gate_sum)) * up_sum
                ).astype(bf16)
                return carry

            lax.fori_loop(0, hidden_units // tile, one_tile, 0)

        def down(half, shard):
            return jnp.dot(
                hidden[pl.ds(half * half_rows, half_rows)],
                down_v[:, pl.ds(pl.multiple_of(shard * width, width), width)],
                preferred_element_type=f32,
            )

        parts, sums = {}, {}

        def shrink(half):
            for step in list(range(1, lines)) + [0]:
                part_send[half, step] = down(half, line_at(step) * 2 + 1 - core).astype(bf16)
                parts[half, step] = push(
                    part_send.at[half, step], part_pair.at[half, step], part_sem, (half, step),
                    {"tp": partner},
                )
            for step in range(1, lines):
                other_sum[half, step - 1] = down(half, line_at(step) * 2 + core)
            own_sum[half] = down(half, me_t)

        def join(half):
            for step in range(1, lines):
                parts[half, step].wait_recv()
                sum_send[half, step - 1] = (
                    other_sum[half, step - 1] + part_pair[half, step].astype(f32)
                ).astype(bf16)
                sums[half, step] = push(
                    sum_send.at[half, step - 1], sum_recv.at[half, step - 1], sum_sem,
                    (half, step - 1), {"tp": line_at(step) * 2 + core},
                )

        backs = {}

        def finish(half):
            parts[half, 0].wait_recv()
            value = own_sum[half] + part_pair[half, 0].astype(f32)
            for step in range(1, lines):
                sums[half, step].wait_recv()
                value = value + sum_recv[half, step - 1].astype(f32)
            value = value.astype(bf16)
            result[pl.ds(half * half_rows, half_rows)] = value
            first = half * (experts // halves)
            if half == 0:
                returned[pl.ds(0, capacity)] = value[:capacity]
            for step in range(max(first, 1), first + experts // halves):
                rows = pl.ds(step * capacity, capacity)
                backs[step] = push(
                    result.at[rows], returned.at[rows], back_sem, (step,),
                    {"sp": lax.rem(me_s + experts - step, experts)},
                )

        forward(0)
        forward(1)
        relay(0)
        for load in loads[:2]:
            load.wait()
        settle(0)
        expand(0)
        forward(2)
        relay(1)
        loads[2].wait()
        shrink(0)
        forward(3)
        settle(1)
        join(0)
        expand(1)
        relay(2)
        shrink(1)
        settle(2)
        join(1)
        finish(0)
        expand(2)
        relay(3)
        shrink(2)
        settle(3)
        join(2)
        finish(1)
        expand(3)
        shrink(3)
        join(3)
        finish(2)
        finish(3)
        slot_index = lax.broadcasted_iota(jnp.int32, (token_count, row_total), 1)
        choose = [
            jnp.where(slot_index == at_ref[:, k : k + 1], 1.0, 0.0).astype(bf16)
            for k in range(TOPK)
        ]
        for step in range(1, experts):
            backs[step].wait_recv()
        second_sum = residual_scale * normed.astype(f32)
        back_rows = returned[...]
        for k in range(TOPK):
            second_sum = second_sum + rw_ref[:, k : k + 1] * jnp.dot(
                choose[k], back_rows, preferred_element_type=f32
            )
        out_ref[...] = normalize(second_sum, last_gain_ref[...], 1).astype(bf16)
        for copy in sent:
            copy.wait_send()

    vmem = pl.BlockSpec(memory_space=pltpu.VMEM)
    hbm = pl.BlockSpec(memory_space=pl.ANY)
    dma = pltpu.SemaphoreType.DMA
    other = max(lines - 1, 1)
    return pl.pallas_call(
        kernel,
        out_shape=jax.ShapeDtypeStruct((token_count, width), bf16),
        in_specs=[vmem] * 7 + [hbm] * 3 + [vmem],
        out_specs=vmem,
        scratch_shapes=[
            pltpu.VMEM(gate_weight.shape[1:], bf16),
            pltpu.VMEM(up_weight.shape[1:], bf16),
            pltpu.VMEM(down_weight.shape[1:], bf16),
            dma((3,)),
            pltpu.VMEM((lines, token_count, width), bf16),
            pltpu.VMEM((lines, token_count, width), bf16),
            pltpu.VMEM((other, token_count, width), bf16),
            pltpu.VMEM((other, token_count, width), bf16),
            dma((2, lines)),
            dma((2, other)),
            pltpu.VMEM((2, 8, token_count), f32),
            pltpu.VMEM((2, shards - 1, 8, token_count), f32),
            dma((2, 2, shards - 1)),
            pltpu.VMEM((row_total, width), bf16),
            pltpu.VMEM((shards, row_total, width), bf16),
            dma((2, experts)),
            dma((2, groups)),
            dma((2, groups, other)),
            dma((2, groups, other)),
            pltpu.VMEM((row_total, hidden_units), bf16),
            pltpu.VMEM((halves, lines, half_rows, width), bf16),
            pltpu.VMEM((halves, lines, half_rows, width), bf16),
            pltpu.VMEM((halves, other, half_rows, width), bf16),
            pltpu.VMEM((halves, other, half_rows, width), bf16),
            pltpu.VMEM((halves, half_rows, width), f32),
            pltpu.VMEM((halves, other, half_rows, width), f32),
            dma((2, halves, lines)),
            dma((2, halves, other)),
            pltpu.VMEM((row_total, width), bf16),
            pltpu.VMEM((row_total, width), bf16),
            dma((2, experts)),
        ],
        compiler_params=pltpu.CompilerParams(
            collective_id=1, has_side_effects=True, vmem_limit_bytes=50 << 20
        ),
    )(
        attended, out_weight, residual, norm_gain.reshape(1, -1), places, places_across,
        route_weights, gate_weight, up_weight, down_weight, final_gain.reshape(1, -1),
    )


def per_device(
    queries,
    projected_key_rows,
    projected_value_rows,
    query_gain,
    key_norm_gain,
    residual,
    out_weight,
    norm_gain,
    expert_ids,
    route_weights,
    gate_weight,
    up_weight,
    down_weight,
    final_gain,
):
    token_count = queries.shape[0]
    query_heads = queries.shape[1] // HEAD_DIM
    key_heads = projected_key_rows.shape[1] // HEAD_DIM
    queries_per_group = query_heads // key_heads
    token_positions = lax.axis_index("sp") * token_count + jnp.arange(token_count, dtype=jnp.int32)
    queries_after_rotation = rotary_over_grid(
        normalize_heads(queries, query_gain, query_heads), token_positions
    ).astype(jnp.bfloat16)
    keys_after_rotation = rotary_over_grid(
        normalize_heads(projected_key_rows, key_norm_gain, key_heads), token_positions
    ).astype(jnp.bfloat16)
    packed = jnp.concatenate(
        [keys_after_rotation, projected_value_rows.reshape(token_count, key_heads, HEAD_DIM)], -1
    ).reshape(token_count, key_heads * 2 * HEAD_DIM)
    grouped_query_heads = (
        queries_after_rotation.reshape(token_count, key_heads, queries_per_group, HEAD_DIM)
        .transpose(1, 2, 0, 3)
        .reshape(key_heads, queries_per_group * token_count, HEAD_DIM)
    )
    score_scale = HEAD_DIM ** (-0.5)
    query_total = queries_per_group * token_count
    group = lax.axis_size("sp")
    section = ring_gather(packed, group, 1 << ((group.bit_length() - 1) // 2)).reshape(
        group * token_count, packed.shape[1]
    )
    running_max = jnp.full((key_heads, query_total), far_below, jnp.float32)
    opened = section.reshape(section.shape[0], key_heads, 2 * HEAD_DIM)
    scores = (
        jnp.einsum(
            "hqd,khd->hqk",
            grouped_query_heads,
            opened[:, :, :HEAD_DIM],
            preferred_element_type=jnp.float32,
        )
        * score_scale
    )
    new_peak = jnp.maximum(running_max, jnp.max(scores, -1))
    weights = jnp.exp(scores - new_peak[:, :, None])
    running_sum = jnp.sum(weights, -1)
    running_out = jnp.einsum(
        "hqk,khd->hqd",
        weights.astype(jnp.bfloat16),
        opened[:, :, HEAD_DIM:],
        preferred_element_type=jnp.float32,
    )
    running_max, running_sum, running_out = (new_peak, running_sum, running_out)
    attended = (running_out / running_sum[:, :, None]).astype(jnp.bfloat16)
    attended = (
        attended.reshape(key_heads, queries_per_group, token_count, HEAD_DIM)
        .transpose(2, 0, 1, 3)
        .reshape(token_count, query_heads * HEAD_DIM)
    )
    expert_count = group
    capacity = 4 * token_count // expert_count
    marked = (
        expert_ids[:, :, None] == jnp.arange(expert_count, dtype=jnp.int32)[None, None, :]
    ).astype(jnp.float32)
    token_index = jnp.arange(token_count, dtype=jnp.int32)
    before = (token_index[None, :] < token_index[:, None]).astype(jnp.bfloat16)
    earlier = jnp.dot(
        before, jnp.sum(marked, 1).astype(jnp.bfloat16), preferred_element_type=jnp.float32
    )
    slots = jnp.sum(earlier[:, None, :] * marked, 2).astype(jnp.int32)
    away = lax.rem(expert_ids - lax.axis_index("sp") + expert_count, expert_count)
    places = away * capacity + slots
    return after_attention(
        attended,
        out_weight,
        residual,
        norm_gain,
        places,
        route_weights,
        gate_weight,
        up_weight,
        down_weight,
        final_gain,
        expert_count,
        lax.axis_size("tp"),
    )


def solution(mesh):
    in_specs = (
        P("sp", "tp"),
        P("sp", "tp"),
        P("sp", "tp"),
        P(),
        P(),
        P("sp", "tp"),
        P("tp", None),
        P("tp"),
        P("sp", None),
        P("sp", None),
        P("sp", None, "tp"),
        P("sp", None, "tp"),
        P("sp", "tp", None),
        P("tp"),
    )
    out_specs = P("sp", "tp")
    return jax.shard_map(
        per_device, mesh=mesh, in_specs=in_specs, out_specs=out_specs, check_vma=False
    )
```

profile of v0, /device:TPU:0, one launch (start us, length us, event | category | flops | bytes accessed | tf_op | source)
XLA Modules:
  0.0 87.7 jit_solution(16024964141219164396)
XLA Ops:
  0.0 0.1 multiply_cosine_fusion
  0.2 1.0 %copy.37 = bf16[128,256]{0,1:T(8,128)(2,1)S(1)} copy(bf16[128,256]{1,0:T(8,128)(2,1)} %param.15) | data formatting | bytes 131072 | tf_op args[1]
  1.2 0.7 fusion.21
  1.9 0.0 copy-start.4
  2.0 0.0 copy-start.7
  2.0 1.0 %copy.38 = bf16[128,256]{0,1:T(8,128)(2,1)S(1)} copy(bf16[128,256]{1,0:T(8,128)(2,1)} %param.16) | data formatting | bytes 131072 | tf_op args[2]
  3.0 0.1 copy.46.mine_ref
  3.1 19.6 %shard_map.136 = bf16[8,128,512]{2,1,0:T(8,128)(2,1)S(1)} custom-call(bf16[128,512]{1,0:T(8,128)(2,1)S(1)} %copy.46.mine_ref), custom_call_target="tpu_custom_call" | custom-call | tf_op jit(solution)/shard_map/pallas_call | solution.py:129
  22.7 0.3 reshape_reshape.3
  23.0 0.9 %fusion.36 = (bf16[1024,4,64]{2,1,0:T(4,128)(2,1)S(1)}, bf16[1024,4,64]{2,1,0:T(4,128)(2,1)S(1)}) fusion(bf16[1024,4,128]{2,1,0:T(4,128)(2,1)S(1)} %reshape_reshape.3), kind=kLoop, calls=%fused_computation.66 | loop fusion | bytes 2097152 | tf_op jit(solution)/shard_map/slice | solution.py:541
  24.0 0.0 copy-done.4
  24.0 0.1 copy.35
  24.2 0.0 copy-done.7
  24.2 0.1 fusion.19
  24.3 0.9 multiply_reduce_fusion
  25.2 0.9 %fusion = f32[4,256]{1,0:T(4,128)S(1)} fusion(f32[4,256,1024]{2,1,0:T(8,128)S(1)} %get-tuple-element.20, f32[4,256]{1,0:T(4,128)S(1)} %broadcast_maximum_fusion), kind=kLoop, calls=%fused_computation.2 | loop fusion | flops 3144704 | bytes 4202496 | tf_op jit(solution)/shard_map/reduce_sum | solution.py:537
  26.1 0.0 copy-start.6
  26.1 0.0 copy-start
  26.1 0.0 copy-start.1
  26.1 0.0 copy-start.2
  26.1 0.0 copy-start.3
  26.1 1.0 %fusion.12 = bf16[4,8,2,8,128]{4,3,2,1,0:T(8,128)(2,1)S(1)} fusion(f32[4,256,1024]{2,1,0:T(8,128)S(1)} %get-tuple-element.20, f32[4,256]{1,0:T(4,128)S(1)} %broadcast_maximum_fusion, bf16[1024,4,64]{2,1,0:T(4,128)(2,1)S(1)} %get-tuple-element.5, f32[4,256]{1,0:T(4,128)S(1)} %fusion), kind=kOutput, calls=%fused_computation.9 | convolution fusion | flops 137494528 | bytes 4857856 | tf_op jit(solution)/shard_map/hqk,khd->hqd/dot_general | solution.py:538
  27.1 0.1 copy.43.att_ref
  27.3 0.0 copy-done.5
  27.3 0.1 fusion.24
  27.5 0.1 copy.44.at_ref
  27.6 0.0 copy-done.6
  27.6 0.1 copy.45.rw_ref
  27.7 0.0 copy-done
  27.7 0.0 copy-done.1
  27.7 59.3 %shard_map.137 = bf16[128,512]{1,0:T(8,128)(2,1)S(1)} custom-call(bf16[128,512]{1,0:T(8,128)(2,1)S(1)} %copy.43.att_ref, bf16[512,2048]{1,0:T(8,128)(2,1)S(1)} %copy-done, bf16[128,512]{1,0:T(8,128)(2,1)S(1)} %copy-done.1, f32[1,512]{1,0:T(1,128)S(1)} %bitcast.37, s32[128,2]{1,0:T(8,128)S(1)} %copy.44.at_ref, s32[2,128]{1,0:T(2,128)S(1)} %bitcast.36, ...), custom_call_target="tpu_custom_call" | custom-call | tf_op jit(solution)/shard_map/pallas_call | solution.py:436
  87.0 0.7 copy.70
  (20 shorter events, 0.3 us)
Async XLA Ops:
  1.9 22.1 %copy-start.4 = (bf16[128,512]{1,0:T(8,128)(2,1)S(1)}, bf16[128,512]{1,0:T(8,128)(2,1)}, u32[]{:S(2)}) copy-start(bf16[128,512]{1,0:T(8,128)(2,1)} %param.14) | copy-start | bytes 393220
  2.0 22.2 %copy-start.7 = (f32[64]{0:T(128)S(1)}, f32[64]{0:T(128)}, u32[]{:S(2)}) copy-start(f32[64]{0:T(128)} %param.17) | copy-start | bytes 772
  26.1 1.2 %copy-start.5 = (s32[128,2]{0,1:T(2,128)S(1)}, s32[128,2]{0,1:T(2,128)}, u32[]{:S(2)}) copy-start(s32[128,2]{0,1:T(2,128)} %param.22) | copy-start | bytes 3076
  26.1 1.5 %copy-start.6 = (f32[128,2]{0,1:T(2,128)S(1)}, f32[128,2]{0,1:T(2,128)}, u32[]{:S(2)}) copy-start(f32[128,2]{0,1:T(2,128)} %param.23) | copy-start | bytes 3076
  26.1 1.6 %copy-start = (bf16[512,2048]{1,0:T(8,128)(2,1)S(1)}, bf16[512,2048]{1,0:T(8,128)(2,1)}, u32[]{:S(2)}) copy-start(bf16[512,2048]{1,0:T(8,128)(2,1)} %ow_ref.1) | copy-start | bytes 6291460
  26.1 1.6 %copy-start.1 = (bf16[128,512]{1,0:T(8,128)(2,1)S(1)}, bf16[128,512]{1,0:T(8,128)(2,1)}, u32[]{:S(2)}) copy-start(bf16[128,512]{1,0:T(8,128)(2,1)} %res_ref.1) | copy-start | bytes 393220
  26.1 1.6 %copy-start.2 = (f32[512]{0:T(512)S(1)}, f32[512]{0:T(512)}, u32[]{:S(2)}) copy-start(f32[512]{0:T(512)} %param.21) | copy-start | bytes 6148
  26.1 1.6 %copy-start.3 = (f32[512]{0:T(512)S(1)}, f32[512]{0:T(512)}, u32[]{:S(2)}) copy-start(f32[512]{0:T(512)} %param.27) | copy-start | bytes 6148
where the time goes:
time: 87.9 us; the launch traced here: 87.7 us
  Pallas kernels  78.9 us (90%)
  local copies, waits for them, and re-layouts  4.46 us (5%)
  other arithmetic  2.1 us (2%)
  matrix products  1.94 us (2%)
    pallas_call x1, Pallas kernels, after_attention(): pl.pallas_call(kernel, out_shape=jax.ShapeDtypeStruct((token_count, width...  59.3 us
    pallas_call x1, Pallas kernels, ring_gather(): pl.pallas_call(kernel, out_shape=jax.ShapeDtypeStruct((group, rows, width...  19.6 us
    unnamed x21, local copies, waits for them, and re-layouts  2.84 us

commit v1 on v0

v1 whole, which is shorter than its diff:
```python
import contextlib

import jax
import jax.numpy as jnp
import numpy as np
from jax import lax
from jax.experimental import pallas as pl
from jax.experimental.pallas import tpu as pltpu
from jax.sharding import PartitionSpec as P

D = 2048
HEAD_DIM = 64
GRID_W = 64
TOPK = 2


theta_base = 10000.0
norm_epsilon = 1e-06
residual_scale = 8.0**0.25
far_below = -1e30
MESH = pl.DeviceIdType.MESH
SCOPES = False


def scope(name):
    return jax.named_scope(name) if SCOPES else contextlib.nullcontext()


def rotary_tables(grid_rows):
    quarter = HEAD_DIM // 4
    lane = np.arange(2 * HEAD_DIM)
    frequency = theta_base ** (-(lane % quarter) * 2.0 / (HEAD_DIM // 2))
    sign = np.where(lane % (2 * quarter) < quarter, -1.0, 1.0)
    by_row = lane % HEAD_DIM < HEAD_DIM // 2

    def tables(positions):
        angles = positions[:, None] * frequency[None, :].astype(np.float32).astype(np.float64)
        return np.stack([np.cos(angles), np.sin(angles) * sign[None, :]]).astype(np.float32)

    rows = np.where(by_row[None, None, :], tables(np.arange(grid_rows)), 0.0)
    columns = np.where(by_row[None, None, :], 0.0, tables(np.arange(GRID_W)))
    return rows.astype(np.float32), columns.astype(np.float32)


def place_of(index, group, group_minor):
    major = group // group_minor
    high, low = index // group_minor, lax.rem(index, group_minor)
    if group_minor == 1:
        return high
    back = major - 1 - high
    odd = lax.rem(back, 2)
    inner = (low - 1) * (1 - odd) + (group_minor - 1 - low) * odd
    first = jnp.where(low == 0, 1, 0)
    return first * high + (1 - first) * (major + back * (group_minor - 1) + inner)


def device_at(place, group, group_minor):
    major = group // group_minor
    if group_minor == 1:
        return place
    first = jnp.where(place < major, 1, 0)
    rest = jnp.maximum(place - major, 0)
    back = rest // (group_minor - 1)
    inner = lax.rem(rest, group_minor - 1)
    odd = lax.rem(back, 2)
    low = 1 + inner * (1 - odd) + (group_minor - 2 - inner) * odd
    other = (major - 1 - back) * group_minor + low
    return first * (place * group_minor) + (1 - first) * other


def layer(
    queries, key_rows, value_rows, row_table, column_table, query_gain, key_gain, out_weight, residual,
    norm_gain, expert_ids, route_weights, gate_weight, up_weight, down_weight, final_gain, experts,
    shards,
):
    token_count, width = residual.shape
    key_heads = key_rows.shape[1] // HEAD_DIM
    pair_width = 2 * HEAD_DIM
    query_rows = 2 * token_count
    ring_minor = 1 << ((experts.bit_length() - 1) // 2)
    ring_half = experts // 2
    pieces = 4
    piece = token_count // pieces
    lines = shards // 2
    row_total = TOPK * 2 * token_count
    capacity = row_total // experts
    groups = 4
    group_rows = row_total // groups
    group_experts = experts // groups
    halves = groups
    half_rows = row_total // halves
    hidden_units = gate_weight.shape[2]
    tile = min(256, hidden_units)
    feature_total = width * shards
    bf16, f32 = jnp.bfloat16, jnp.float32

    def kernel(
        row_hbm, column_hbm, q_gain_hbm, k_gain_hbm, gain_hbm, ids_hbm, rw_hbm, last_gain_hbm,
        q_hbm, k_hbm, v_hbm, res_hbm, ow_hbm, gate_hbm, up_hbm, down_hbm, out_ref,
        row_ref, column_ref, q_gain_ref, k_gain_ref, gain_ref, ids_ref, rw_ref, last_gain_ref,
        small_sem, q_v, k_v, v_v, res_ref, ow_ref, gate_v, up_v, down_v, weight_sem,
        ring_ref, ring_send, ring_recv, q_pad, flash_out, flash_max, flash_sum, att_ref,
        mix_send, mix_pair, line_send, line_recv, mix_sem, line_sem,
        stat_send, stat_recv, stat_sem,
        outgoing, routed, out_sem, fwd_sem, cross_sem, relay_sem,
        hidden, part_send, part_pair, sum_send, sum_recv, own_sum, other_sum, part_sem, sum_sem,
        result, returned, back_sem,
    ):
        me_s = lax.axis_index("sp")
        me_t = lax.axis_index("tp")
        line = me_t // 2
        core = lax.rem(me_t, 2)
        partner = line * 2 + 1 - core

        def line_at(step):
            return lax.rem(line + step, lines)

        barrier = pltpu.get_barrier_semaphore()
        for step in range(1, experts):
            pl.semaphore_signal(
                barrier, inc=1, device_id={"sp": lax.rem(me_s + step, experts)},
                device_id_type=MESH,
            )
        for step in range(1, shards):
            pl.semaphore_signal(
                barrier, inc=1, device_id={"tp": lax.rem(me_t + step, shards)},
                device_id_type=MESH,
            )
        loads = [
            pltpu.make_async_copy(src, dst, weight_sem.at[i])
            for i, (src, dst) in enumerate(
                (
                    (k_hbm, k_v), (v_hbm, v_v), (q_hbm, q_v), (ow_hbm, ow_ref), (res_hbm, res_ref),
                    (gate_hbm.at[0], gate_v), (up_hbm.at[0], up_v), (down_hbm.at[0], down_v),
                )
            )
        ]
        small_loads = [
            pltpu.make_async_copy(src, dst, small_sem.at[i])
            for i, (src, dst) in enumerate(
                (
                    (row_hbm, row_ref), (column_hbm, column_ref), (q_gain_hbm, q_gain_ref),
                    (k_gain_hbm, k_gain_ref), (gain_hbm, gain_ref), (ids_hbm, ids_ref),
                    (rw_hbm, rw_ref), (last_gain_hbm, last_gain_ref),
                )
            )
        ]
        for load in loads[:3] + small_loads + loads[3:]:
            load.start()
        sent = []

        def push(source, target, sems, index, device):
            copy = pltpu.make_async_remote_copy(
                src_ref=source, dst_ref=target,
                send_sem=sems.at[(0,) + index], recv_sem=sems.at[(1,) + index],
                device_id=device, device_id_type=MESH,
            )
            copy.start()
            sent.append(copy)
            return copy

        lane_pair = lax.broadcasted_iota(jnp.int32, (token_count, pair_width), 1)
        low_half = lane_pair < HEAD_DIM
        quarter = HEAD_DIM // 4
        turn_low = lane_pair % (2 * quarter) < quarter
        same_head = jnp.where(
            lax.broadcasted_iota(jnp.int32, (pair_width, pair_width), 0) // HEAD_DIM
            == lax.broadcasted_iota(jnp.int32, (pair_width, pair_width), 1) // HEAD_DIM,
            1.0, 0.0,
        ).astype(bf16)
        for load in small_loads:
            load.wait()

        def rotary(part):
            blocks = []
            for line_of_grid in range(token_count // GRID_W):
                row = row_ref[part, pl.ds(me_s * (token_count // GRID_W) + line_of_grid, 1)]
                blocks.append(column_ref[part] + row)
            return jnp.concatenate(blocks, 0)

        cosine, sine = rotary(0), rotary(1)
        both_gains = [
            jnp.concatenate([ref[...]] * 2, 1) for ref in (q_gain_ref, k_gain_ref)
        ]

        def rotated(rows, gain):
            square = rows * rows
            high = square.astype(bf16)
            rest = (square - high.astype(f32)).astype(bf16)
            total = jnp.dot(high, same_head, preferred_element_type=f32) + jnp.dot(
                rest, same_head, preferred_element_type=f32
            )
            scaled = rows * lax.rsqrt(total / HEAD_DIM + norm_epsilon) * gain
            turned = jnp.where(
                turn_low,
                pltpu.roll(scaled, pair_width - quarter, 1),
                pltpu.roll(scaled, quarter, 1),
            )
            return scaled * cosine + turned * sine

        def swap(rows):
            return pltpu.roll(rows, HEAD_DIM, 1)

        loads[0].wait()
        loads[1].wait()
        for pair in range((key_heads + 1) // 2):
            if key_heads == 1:
                key_pair = jnp.concatenate([k_v[...]] * 2, 1).astype(f32)
                value_pair = jnp.concatenate([v_v[...]] * 2, 1).astype(f32)
            else:
                lanes = pl.ds(pair * pair_width, pair_width)
                key_pair = k_v[:, lanes].astype(f32)
                value_pair = v_v[:, lanes].astype(f32)
            key_pair = rotated(key_pair, both_gains[1])
            ring_ref[0, :, pl.ds(2 * pair * pair_width, pair_width)] = jnp.where(
                low_half, key_pair, swap(value_pair)
            ).astype(bf16)
            if key_heads > 1:
                ring_ref[0, :, pl.ds((2 * pair + 1) * pair_width, pair_width)] = jnp.where(
                    low_half, swap(key_pair), value_pair
                ).astype(bf16)
        spot = place_of(me_s, experts, ring_minor)
        right = device_at(lax.rem(spot + 1, experts), experts, ring_minor)
        left = device_at(lax.rem(spot + experts - 1, experts), experts, ring_minor)
        with scope("barrier"):
            pl.semaphore_wait(barrier, experts + shards - 2)

        ring = {}

        def pass_on(hop, part):
            for way in range(2):
                if hop == ring_half and (part < pieces // 2) != (way == 0):
                    continue
                if hop > 1:
                    ring[way, hop - 1, part].wait_recv()
                span = pl.ds(part * piece, piece)
                source_slot = (hop - 1) if way == 0 else (experts - hop + 1) % experts
                target_slot = hop if way == 0 else experts - hop
                copy = pltpu.make_async_remote_copy(
                    src_ref=ring_ref.at[source_slot, span], dst_ref=ring_ref.at[target_slot, span],
                    send_sem=ring_send.at[way, hop - 1, part],
                    recv_sem=ring_recv.at[way, hop - 1, part],
                    device_id={"sp": right if way == 0 else left}, device_id_type=MESH,
                )
                copy.start()
                sent.append(copy)
                ring[way, hop, part] = copy

        def attend(slot, head, first):
            block = ring_ref[slot, :, pl.ds(head * pair_width, pair_width)]
            scores = lax.dot_general(
                block, q_pad[head], (((1,), (1,)), ((), ())), preferred_element_type=f32
            )
            peak = jnp.max(scores, 0, keepdims=True)
            if not first:
                peak = jnp.maximum(flash_max[head], peak)
            weights = jnp.exp(scores - peak)
            mass = jnp.sum(weights, 0, keepdims=True)
            gathered = lax.dot_general(
                block, weights.astype(bf16), (((0,), (0,)), ((), ())), preferred_element_type=f32
            )[HEAD_DIM:]
            if not first:
                fade = jnp.exp(flash_max[head] - peak)
                mass = mass + flash_sum[head] * fade
                gathered = gathered + flash_out[head] * fade
            flash_max[head] = peak
            flash_sum[head] = mass
            flash_out[head] = gathered

        def prepare(head):
            rows = rotated(
                q_v[:, pl.ds(head * pair_width, pair_width)].astype(f32), both_gains[0]
            ) * HEAD_DIM ** (-0.5)
            q_pad[head, pl.ds(0, token_count)] = jnp.where(low_half, rows, 0.0).astype(bf16)
            q_pad[head, pl.ds(token_count, token_count)] = jnp.where(
                low_half, swap(rows), 0.0
            ).astype(bf16)

        waiting = []
        for part in range(pieces):
            pass_on(1, part)
        loads[2].wait()
        for head in range(key_heads):
            prepare(head)
        waiting += [(0, head, True) for head in range(key_heads)]
        for hop in range(2, ring_half + 1):
            for part in range(pieces):
                pass_on(hop, part)
                for _ in range(-(-len(waiting) // (pieces - part))):
                    attend(*waiting.pop(0))
            if hop < ring_half:
                for slot in (hop - 1, experts - hop + 1):
                    waiting += [(slot, head, False) for head in range(key_heads)]
        with scope("ring_tail"):
            for way in range(2):
                for part in range(pieces):
                    if (way, ring_half, part) not in ring:
                        ring[way, ring_half - 1, part].wait_recv()
        for slot in (ring_half - 1, ring_half + 1):
            for head in range(key_heads):
                attend(slot, head, False)
        with scope("ring_last"):
            for way in range(2):
                for part in range(pieces):
                    if (way, ring_half, part) in ring:
                        ring[way, ring_half, part].wait_recv()
        for head in range(key_heads):
            attend(ring_half, head, False)
            result_rows = flash_out[head] / flash_sum[head]
            att_ref[:, pl.ds(head * pair_width, pair_width)] = (
                jnp.concatenate([result_rows[:, :token_count], result_rows[:, token_count:]], 0)
                .T.astype(bf16)
            )
        attended_rows = att_ref[...]
        loads[3].wait()

        def mix(shard):
            return jnp.dot(
                attended_rows,
                ow_ref[:, pl.ds(pl.multiple_of(shard * width, width), width)],
                preferred_element_type=f32,
            )

        for step in range(lines):
            mix_send[step] = mix(line_at(step) * 2 + 1 - core).astype(bf16)
        pair = {}
        for step in list(range(1, lines)) + [0]:
            pair[step] = push(
                mix_send.at[step], mix_pair.at[step], mix_sem, (step,), {"tp": partner}
            )
        across = {}
        for step in range(1, lines):
            mine = mix(line_at(step) * 2 + core)
            pair[step].wait_recv()
            line_send[step - 1] = (mine + mix_pair[step].astype(f32)).astype(bf16)
            across[step] = push(
                line_send.at[step - 1], line_recv.at[step - 1], line_sem, (step - 1,),
                {"tp": line_at(step) * 2 + core},
            )
        total = mix(me_t)
        pair[0].wait_recv()
        total = total + mix_pair[0].astype(f32)
        loads[4].wait()
        total = total + residual_scale * res_ref[...].astype(f32)
        for step in range(1, lines):
            across[step].wait_recv()
            total = total + line_recv[step - 1].astype(f32)

        lane = lax.broadcasted_iota(jnp.int32, (token_count, 128), 1)

        before = jnp.where(
            lax.broadcasted_iota(jnp.int32, (token_count, token_count), 1)
            < lax.broadcasted_iota(jnp.int32, (token_count, token_count), 0),
            1.0, 0.0,
        ).astype(bf16)

        def columns_of(rows):
            return jnp.concatenate([rows] * (token_count // TOPK), 0).T

        ids = columns_of(ids_ref[...].astype(f32)).astype(jnp.int32)
        routing = columns_of(rw_ref[...])
        marked = [jnp.where(lane == ids[:, k : k + 1], 1.0, 0.0) for k in range(TOPK)]
        earlier = jnp.dot(before, (marked[0] + marked[1]).astype(bf16), preferred_element_type=f32)
        at = []
        for k in range(TOPK):
            away = lax.rem(ids[:, k : k + 1] - me_s + experts, experts)
            at.append(
                (away * capacity).astype(f32) + jnp.sum(earlier * marked[k], 1, keepdims=True)
            )
        across = jnp.where(lane == 0, at[0], jnp.where(lane == 1, at[1], 0.0)).T.astype(jnp.int32)
        at = [column.astype(jnp.int32) for column in at]

        def normalize(values, gain, turn):
            sums = jnp.sum(values, 1, keepdims=True)
            squares = jnp.sum(values * values, 1, keepdims=True)
            both = jnp.where(lane == 0, sums, jnp.where(lane == 1, squares, 0.0)).T[:8]
            stat_send[turn] = both
            stats = [
                push(
                    stat_send.at[turn], stat_recv.at[turn, step - 1], stat_sem,
                    (turn, step - 1), {"tp": lax.rem(me_t + step, shards)},
                )
                for step in range(1, shards)
            ]
            for step in range(1, shards):
                stats[step - 1].wait_recv()
                both = both + stat_recv[turn, step - 1]
            columns = jnp.concatenate([both] * 16, 0).T
            center = columns[:, 0:1] / feature_total
            spread = columns[:, 1:2] / feature_total - center * center
            return (values - center) * lax.rsqrt(spread + norm_epsilon) * gain

        normed = normalize(total, gain_ref[...], 0).astype(bf16)
        row_index = lax.broadcasted_iota(jnp.int32, (row_total, token_count), 0)
        picks = jnp.where(
            (row_index == across[0:1, :]) | (row_index == across[1:2, :]), 1.0, 0.0
        ).astype(bf16)
        spread_rows = jnp.dot(picks, normed, preferred_element_type=f32).astype(bf16)
        outgoing[...] = spread_rows
        routed[me_t, pl.ds(0, capacity)] = spread_rows[:capacity]
        arrivals = {}
        for step in range(1, experts):
            rows = pl.ds(step * capacity, capacity)
            arrivals[step] = push(
                outgoing.at[rows], routed.at[me_t, rows], out_sem, (step,),
                {"sp": lax.rem(me_s + step, experts)},
            )
        forwards, crossings, relays = {}, {}, {}

        def forward(group):
            for step in range(group * group_experts, (group + 1) * group_experts):
                if step > 0:
                    arrivals[step].wait_recv()
            rows = pl.ds(group * group_rows, group_rows)
            block = routed.at[me_t, rows]
            for step in range(1, lines):
                crossings[group, step] = push(
                    block, block, cross_sem, (group, step - 1),
                    {"tp": line_at(step) * 2 + core},
                )
            forwards[group] = push(block, block, fwd_sem, (group,), {"tp": partner})

        def relay(group):
            rows = pl.ds(group * group_rows, group_rows)
            for step in range(1, lines):
                crossings[group, step].wait_recv()
                block = routed.at[line_at(lines - step) * 2 + core, rows]
                relays[group, step] = push(
                    block, block, relay_sem, (group, step - 1), {"tp": partner}
                )

        def settle(group):
            forwards[group].wait_recv()
            for step in range(1, lines):
                relays[group, step].wait_recv()

        def expand(half):
            rows = pl.ds(half * half_rows, half_rows)

            def one_tile(index, carry):
                cols = pl.ds(pl.multiple_of(index * tile, tile), tile)
                gate_sum = jnp.zeros((half_rows, tile), f32)
                up_sum = jnp.zeros((half_rows, tile), f32)
                for shard in range(shards):
                    block = routed[shard, rows]
                    deep = pl.ds(shard * width, width)
                    gate_sum += jnp.dot(block, gate_v[deep, cols], preferred_element_type=f32)
                    up_sum += jnp.dot(block, up_v[deep, cols], preferred_element_type=f32)
                hidden[rows, cols] = (
                    gate_sum / (1.0 + jnp.exp(-gate_sum)) * up_sum
                ).astype(bf16)
                return carry

            lax.fori_loop(0, hidden_units // tile, one_tile, 0)

        def down(half, shard):
            return jnp.dot(
                hidden[pl.ds(half * half_rows, half_rows)],
                down_v[:, pl.ds(pl.multiple_of(shard * width, width), width)],
                preferred_element_type=f32,
            )

        parts, sums = {}, {}

        def shrink(half):
            for step in list(range(1, lines)) + [0]:
                part_send[half, step] = down(half, line_at(step) * 2 + 1 - core).astype(bf16)
                parts[half, step] = push(
                    part_send.at[half, step], part_pair.at[half, step], part_sem, (half, step),
                    {"tp": partner},
                )
            for step in range(1, lines):
                other_sum[half, step - 1] = down(half, line_at(step) * 2 + core)
            own_sum[half] = down(half, me_t)

        def join(half):
            for step in range(1, lines):
                parts[half, step].wait_recv()
                sum_send[half, step - 1] = (
                    other_sum[half, step - 1] + part_pair[half, step].astype(f32)
                ).astype(bf16)
                sums[half, step] = push(
                    sum_send.at[half, step - 1], sum_recv.at[half, step - 1], sum_sem,
                    (half, step - 1), {"tp": line_at(step) * 2 + core},
                )

        backs = {}

        def finish(half):
            parts[half, 0].wait_recv()
            value = own_sum[half] + part_pair[half, 0].astype(f32)
            for step in range(1, lines):
                sums[half, step].wait_recv()
                value = value + sum_recv[half, step - 1].astype(f32)
            value = value.astype(bf16)
            result[pl.ds(half * half_rows, half_rows)] = value
            first = half * (experts // halves)
            if half == 0:
                returned[pl.ds(0, capacity)] = value[:capacity]
            for step in range(max(first, 1), first + experts // halves):
                rows = pl.ds(step * capacity, capacity)
                backs[step] = push(
                    result.at[rows], returned.at[rows], back_sem, (step,),
                    {"sp": lax.rem(me_s + experts - step, experts)},
                )

        forward(0)
        forward(1)
        relay(0)
        for load in loads[5:7]:
            load.wait()
        settle(0)
        expand(0)
        forward(2)
        relay(1)
        loads[7].wait()
        shrink(0)
        forward(3)
        settle(1)
        join(0)
        expand(1)
        relay(2)
        shrink(1)
        settle(2)
        join(1)
        finish(0)
        expand(2)
        relay(3)
        shrink(2)
        settle(3)
        join(2)
        finish(1)
        expand(3)
        shrink(3)
        join(3)
        finish(2)
        finish(3)
        slot_index = lax.broadcasted_iota(jnp.int32, (token_count, row_total), 1)
        choose = [
            jnp.where(slot_index == at[k], 1.0, 0.0).astype(bf16)
            for k in range(TOPK)
        ]
        for step in range(1, experts):
            backs[step].wait_recv()
        second_sum = residual_scale * normed.astype(f32)
        back_rows = returned[...]
        for k in range(TOPK):
            second_sum = second_sum + routing[:, k : k + 1] * jnp.dot(
                choose[k], back_rows, preferred_element_type=f32
            )
        out_ref[...] = normalize(second_sum, last_gain_ref[...], 1).astype(bf16)
        for copy in sent:
            copy.wait_send()

    vmem = pl.BlockSpec(memory_space=pltpu.VMEM)
    hbm = pl.BlockSpec(memory_space=pltpu.HBM)
    dma = pltpu.SemaphoreType.DMA
    other = max(lines - 1, 1)
    return pl.pallas_call(
        kernel,
        out_shape=jax.ShapeDtypeStruct((token_count, width), bf16),
        in_specs=[hbm] * 16,
        out_specs=vmem,
        scratch_shapes=[
            pltpu.VMEM(row_table.shape, f32),
            pltpu.VMEM(column_table.shape, f32),
            pltpu.VMEM((1, HEAD_DIM), f32),
            pltpu.VMEM((1, HEAD_DIM), f32),
            pltpu.VMEM((1, width), f32),
            pltpu.VMEM((TOPK, token_count), jnp.int32),
            pltpu.VMEM((TOPK, token_count), f32),
            pltpu.VMEM((1, width), f32),
            dma((8,)),
            pltpu.VMEM(queries.shape, bf16),
            pltpu.VMEM(key_rows.shape, bf16),
            pltpu.VMEM(value_rows.shape, bf16),
            pltpu.VMEM(residual.shape, bf16),
            pltpu.VMEM(out_weight.shape, bf16),
            pltpu.VMEM(gate_weight.shape[1:], bf16),
            pltpu.VMEM(up_weight.shape[1:], bf16),
            pltpu.VMEM(down_weight.shape[1:], bf16),
            dma((8,)),
            pltpu.VMEM((experts, token_count, key_heads * pair_width), bf16),
            dma((2, ring_half, pieces)),
            dma((2, ring_half, pieces)),
            pltpu.VMEM((key_heads, query_rows, pair_width), bf16),
            pltpu.VMEM((key_heads, HEAD_DIM, query_rows), f32),
            pltpu.VMEM((key_heads, 1, query_rows), f32),
            pltpu.VMEM((key_heads, 1, query_rows), f32),
            pltpu.VMEM((token_count, key_heads * pair_width), bf16),
            pltpu.VMEM((lines, token_count, width), bf16),
            pltpu.VMEM((lines, token_count, width), bf16),
            pltpu.VMEM((other, token_count, width), bf16),
            pltpu.VMEM((other, token_count, width), bf16),
            dma((2, lines)),
            dma((2, other)),
            pltpu.VMEM((2, 8, token_count), f32),
            pltpu.VMEM((2, shards - 1, 8, token_count), f32),
            dma((2, 2, shards - 1)),
            pltpu.VMEM((row_total, width), bf16),
            pltpu.VMEM((shards, row_total, width), bf16),
            dma((2, experts)),
            dma((2, groups)),
            dma((2, groups, other)),
            dma((2, groups, other)),
            pltpu.VMEM((row_total, hidden_units), bf16),
            pltpu.VMEM((halves, lines, half_rows, width), bf16),
            pltpu.VMEM((halves, lines, half_rows, width), bf16),
            pltpu.VMEM((halves, other, half_rows, width), bf16),
            pltpu.VMEM((halves, other, half_rows, width), bf16),
            pltpu.VMEM((halves, half_rows, width), f32),
            pltpu.VMEM((halves, other, half_rows, width), f32),
            dma((2, halves, lines)),
            dma((2, halves, other)),
            pltpu.VMEM((row_total, width), bf16),
            pltpu.VMEM((row_total, width), bf16),
            dma((2, experts)),
        ],
        compiler_params=pltpu.CompilerParams(
            collective_id=0, has_side_effects=True, vmem_limit_bytes=58 << 20
        ),
    )(
        row_table, column_table, query_gain.reshape(1, -1), key_gain.reshape(1, -1),
        norm_gain.reshape(1, -1), expert_ids.T, route_weights.T,
        final_gain.reshape(1, -1), queries, key_rows, value_rows, residual, out_weight,
        gate_weight, up_weight, down_weight,
    )


def per_device(
    queries,
    projected_key_rows,
    projected_value_rows,
    query_gain,
    key_norm_gain,
    residual,
    out_weight,
    norm_gain,
    expert_ids,
    route_weights,
    gate_weight,
    up_weight,
    down_weight,
    final_gain,
):
    token_total = queries.shape[0] * lax.axis_size("sp")
    row_table, column_table = rotary_tables(-(-token_total // GRID_W))
    return layer(
        queries,
        projected_key_rows,
        projected_value_rows,
        row_table,
        column_table,
        query_gain,
        key_norm_gain,
        out_weight,
        residual,
        norm_gain,
        expert_ids,
        route_weights,
        gate_weight,
        up_weight,
        down_weight,
        final_gain,
        lax.axis_size("sp"),
        lax.axis_size("tp"),
    )


def solution(mesh):
    in_specs = (
        P("sp", "tp"),
        P("sp", "tp"),
        P("sp", "tp"),
        P(),
        P(),
        P("sp", "tp"),
        P("tp", None),
        P("tp"),
        P("sp", None),
        P("sp", None),
        P("sp", None, "tp"),
        P("sp", None, "tp"),
        P("sp", "tp", None),
        P("tp"),
    )
    out_specs = P("sp", "tp")
    return jax.shard_map(
        per_device, mesh=mesh, in_specs=in_specs, out_specs=out_specs, check_vma=False
    )
```

time: 87.9 us -> 82.3 us (0.936)
  local copies, waits for them, and re-layouts: 4.46 us -> 1.57 us
  other arithmetic: 2.1 us -> 0 us
  matrix products: 1.94 us -> 0 us
  Pallas kernels: 78.9 us -> 80.6 us
    dot_general x3 -> x0, matrix products: 1.94 us -> none  [the longest x1 0.95 us: per_device(): jnp.einsum('hqk,khd->hqd', weights.astype(jnp.bfloat16), opened[:, :, HEA...]
    pallas_call x2 -> x1, Pallas kernels: 78.9 us -> 80.6 us  [layer(): pl.pallas_call(kernel, out_shape=jax.ShapeDtypeStruct((token_count, width...]
    unnamed x21 -> x1, local copies, waits for them, and re-layouts: 2.84 us -> 1.57 us
    reduce_sum x5 -> x0, other arithmetic: 0.98 us -> none  [the longest x1 0.88 us: per_device(): running_sum = jnp.sum(weights, -1)]
    slice x1 -> x0, local copies, waits for them, and re-layouts: 0.95 us -> none  [per_device(): opened[:, :, HEAD_DIM:]]
where the time goes in v1:
time: 82.3 us; the launch traced here: 82.2 us
  Pallas kernels  80.6 us (98%)
  local copies, waits for them, and re-layouts  1.57 us (2%)
    pallas_call x1, Pallas kernels, layer(): pl.pallas_call(kernel, out_shape=jax.ShapeDtypeStruct((token_count, width...  80.6 us

profile of v1, /device:TPU:0, one launch (start us, length us, event | category | flops | bytes accessed | tf_op | source)
XLA Modules:
  0.0 82.2 jit_solution(14697401493197355487)
XLA Ops:
  0.0 80.6 %shard_map.154 = bf16[128,512]{1,0:T(8,128)(2,1)} custom-call(f32[2,16,128]{2,1,0:T(8,128)} %constant.4.clone.row_hbm, f32[2,64,128]{2,1,0:T(8,128)} %constant.5.clone.column_hbm, f32[1,64]{1,0:T(1,128)} %bitcast.10, f32[1,64]{1,0:T(1,128)} %bitcast.11, f32[1,512]{1,0:T(1,128)} %bitcast.6, s32[2,128]{1,0:T(2,128)} %bitcast.8, f32[2,128]{1,0:T(2,128)} %bitcast.9, ...), custom_call_target="tpu_custom_call" | custom-call | tf_op jit(solution)/shard_map/pallas_call | solution.py:559
  80.6 1.6 %copy.18 = bf16[128,512]{1,0:T(8,128)(2,1)} copy(bf16[128,512]{1,0:T(8,128)(2,1)} %shard_map.154) | data formatting | bytes 262144

commit v2 on v1

--- a/solution.py
+++ b/solution.py
@@ -11,6 +11,7 @@
 D = 2048
 HEAD_DIM = 64
 GRID_W = 64
+EXP_GROUP = 4
 TOPK = 2
 
 
@@ -82,13 +83,11 @@
     pieces = 4
     piece = token_count // pieces
     lines = shards // 2
-    row_total = TOPK * 2 * token_count
-    capacity = row_total // experts
-    groups = 4
-    group_rows = row_total // groups
-    group_experts = experts // groups
-    halves = groups
-    half_rows = row_total // halves
+    groups = experts // EXP_GROUP
+    capacity = token_count // groups
+    sets = (1, groups - 1) if groups > 1 else (1,)
+    set_rows = [EXP_GROUP * blocks * capacity for blocks in sets]
+    row_total = sum(set_rows)
     hidden_units = gate_weight.shape[2]
     tile = min(256, hidden_units)
     feature_total = width * shards
@@ -102,10 +101,14 @@
         ring_ref, ring_send, ring_recv, q_pad, flash_out, flash_max, flash_sum, att_ref,
         mix_send, mix_pair, line_send, line_recv, mix_sem, line_sem,
         stat_send, stat_recv, stat_sem,
-        outgoing, routed, out_sem, fwd_sem, cross_sem, relay_sem,
-        hidden, part_send, part_pair, sum_send, sum_recv, own_sum, other_sum, part_sem, sum_sem,
-        result, returned, back_sem,
+        perm_ref, back_ref, weight_send, weight_recv, share_sem, scale_ref, outgoing, hidden,
+        cross_sem, home, returned_ref, back_sem, *per_set,
     ):
+        count = len(sets)
+        (
+            routed, spread_sem, mirror_sem, part_send, part_recv, part_sem, give, take, return_sem,
+            kept,
+        ) = [per_set[i * count : (i + 1) * count] for i in range(10)]
         me_s = lax.axis_index("sp")
         me_t = lax.axis_index("tp")
         line = me_t // 2
@@ -115,6 +118,27 @@
         def line_at(step):
             return lax.rem(line + step, lines)
 
+        me_g = me_s // EXP_GROUP
+        me_m = lax.rem(me_s, EXP_GROUP)
+
+        def member(turn):
+            if turn == 0:
+                return me_m
+            if turn == 1:
+                return me_m + 1 - 2 * lax.rem(me_m, 2)
+            if turn == 2:
+                return me_m + 2 - 4 * (me_m // 2)
+            return EXP_GROUP - 1 - me_m
+
+        def line_before(step):
+            return lax.rem(line + lines - step, lines)
+
+        def group_device(step):
+            return {"sp": lax.rem(me_g + step + groups, groups) * EXP_GROUP + me_m}
+
+        def square_device(turn, step):
+            return {"sp": me_g * EXP_GROUP + member(turn), "tp": line_at(step) * 2 + core}
+
         barrier = pltpu.get_barrier_semaphore()
         for step in range(1, experts):
             pl.semaphore_signal(
@@ -126,6 +150,12 @@
                 barrier, inc=1, device_id={"tp": lax.rem(me_t + step, shards)},
                 device_id_type=MESH,
             )
+        for turn in range(1, EXP_GROUP):
+            for step in range(1, lines):
+                pl.semaphore_signal(
+                    barrier, inc=1, device_id=square_device(turn, step), device_id_type=MESH
+                )
+        greeted = experts - 1 + shards - 1 + (EXP_GROUP - 1) * (lines - 1)
         loads = [
             pltpu.make_async_copy(src, dst, weight_sem.at[i])
             for i, (src, dst) in enumerate(
@@ -223,7 +253,7 @@
         right = device_at(lax.rem(spot + 1, experts), experts, ring_minor)
         left = device_at(lax.rem(spot + experts - 1, experts), experts, ring_minor)
         with scope("barrier"):
-            pl.semaphore_wait(barrier, experts + shards - 2)
+            pl.semaphore_wait(barrier, greeted)
 
         ring = {}
 
@@ -276,12 +306,60 @@
                 low_half, swap(rows), 0.0
             ).astype(bf16)
 
+        def columns_of(rows):
+            return jnp.concatenate([rows] * (token_count // TOPK), 0).T
+
+        lane = lax.broadcasted_iota(jnp.int32, (token_count, 128), 1)
+        before = jnp.where(
+            lax.broadcasted_iota(jnp.int32, (token_count, token_count), 1)
+            < lax.broadcasted_iota(jnp.int32, (token_count, token_count), 0),
+            1.0, 0.0,
+        ).astype(bf16)
+
+        def route():
+            ids = columns_of(ids_ref[...].astype(f32)).astype(jnp.int32)
+            routing = columns_of(rw_ref[...])
+            group_of = ids[:, 0:1] // EXP_GROUP
+            inside = jnp.where(lane == group_of, 1.0, 0.0)
+            earlier = jnp.dot(before, inside.astype(bf16), preferred_element_type=f32)
+            slot = jnp.sum(earlier * inside, 1, keepdims=True)
+            away = lax.rem(group_of - me_g + groups, groups)
+            place = (away * capacity).astype(f32) + slot
+            place_row = jnp.where(lane == 0, place, 0.0).T[0:1].astype(jnp.int32)
+            place = place.astype(jnp.int32)
+            row_index = lax.broadcasted_iota(jnp.int32, (token_count, token_count), 0)
+            picks = jnp.where(row_index == place_row, 1.0, 0.0)
+            perm_ref[...] = picks.astype(bf16)
+            back_ref[...] = jnp.where(
+                lax.broadcasted_iota(jnp.int32, (token_count, token_count), 1) == place, 1.0, 0.0
+            ).astype(bf16)
+            by_expert = sum(
+                jnp.where(lane == ids[:, k : k + 1], routing[:, k : k + 1], 0.0)
+                for k in range(TOPK)
+            )
+            by_slot = jnp.dot(
+                picks, by_expert, preferred_element_type=f32, precision=lax.Precision.HIGHEST
+            ).T
+            for expert in range(experts):
+                weight_send[expert] = jnp.broadcast_to(
+                    by_slot[expert : expert + 1], (8, token_count)
+                )
+            weight_recv[me_s] = weight_send[me_s]
+            return {
+                step: push(
+                    weight_send.at[lax.rem(me_s + step, experts)], weight_recv.at[me_s], share_sem,
+                    (step,), {"sp": lax.rem(me_s + step, experts)},
+                )
+                for step in range(1, experts)
+            }
+
         waiting = []
         for part in range(pieces):
             pass_on(1, part)
         loads[2].wait()
         for head in range(key_heads):
             prepare(head)
+        shares = route()
         waiting += [(0, head, True) for head in range(key_heads)]
         for hop in range(2, ring_half + 1):
             for part in range(pieces):
@@ -321,6 +399,8 @@
                 preferred_element_type=f32,
             )
 
+        with scope("mix"):
+            pass
         for step in range(lines):
             mix_send[step] = mix(line_at(step) * 2 + 1 - core).astype(bf16)
         pair = {}
@@ -345,30 +425,6 @@
         for step in range(1, lines):
             across[step].wait_recv()
             total = total + line_recv[step - 1].astype(f32)
-
-        lane = lax.broadcasted_iota(jnp.int32, (token_count, 128), 1)
-
-        before = jnp.where(
-            lax.broadcasted_iota(jnp.int32, (token_count, token_count), 1)
-            < lax.broadcasted_iota(jnp.int32, (token_count, token_count), 0),
-            1.0, 0.0,
-        ).astype(bf16)
-
-        def columns_of(rows):
-            return jnp.concatenate([rows] * (token_count // TOPK), 0).T
-
-        ids = columns_of(ids_ref[...].astype(f32)).astype(jnp.int32)
-        routing = columns_of(rw_ref[...])
-        marked = [jnp.where(lane == ids[:, k : k + 1], 1.0, 0.0) for k in range(TOPK)]
-        earlier = jnp.dot(before, (marked[0] + marked[1]).astype(bf16), preferred_element_type=f32)
-        at = []
-        for k in range(TOPK):
-            away = lax.rem(ids[:, k : k + 1] - me_s + experts, experts)
-            at.append(
-                (away * capacity).astype(f32) + jnp.sum(earlier * marked[k], 1, keepdims=True)
-            )
-        across = jnp.where(lane == 0, at[0], jnp.where(lane == 1, at[1], 0.0)).T.astype(jnp.int32)
-        at = [column.astype(jnp.int32) for column in at]
 
         def normalize(values, gain, turn):
             sums = jnp.sum(values, 1, keepdims=True)
@@ -390,165 +446,191 @@
             spread = columns[:, 1:2] / feature_total - center * center
             return (values - center) * lax.rsqrt(spread + norm_epsilon) * gain
 
-        normed = normalize(total, gain_ref[...], 0).astype(bf16)
-        row_index = lax.broadcasted_iota(jnp.int32, (row_total, token_count), 0)
-        picks = jnp.where(
-            (row_index == across[0:1, :]) | (row_index == across[1:2, :]), 1.0, 0.0
-        ).astype(bf16)
-        spread_rows = jnp.dot(picks, normed, preferred_element_type=f32).astype(bf16)
+        with scope("norm1"):
+            normed = normalize(total, gain_ref[...], 0).astype(bf16)
+        spread_rows = jnp.dot(perm_ref[...], normed, preferred_element_type=f32).astype(bf16)
         outgoing[...] = spread_rows
-        routed[me_t, pl.ds(0, capacity)] = spread_rows[:capacity]
-        arrivals = {}
-        for step in range(1, experts):
-            rows = pl.ds(step * capacity, capacity)
-            arrivals[step] = push(
-                outgoing.at[rows], routed.at[me_t, rows], out_sem, (step,),
-                {"sp": lax.rem(me_s + step, experts)},
-            )
-        forwards, crossings, relays = {}, {}, {}
-
-        def forward(group):
-            for step in range(group * group_experts, (group + 1) * group_experts):
-                if step > 0:
-                    arrivals[step].wait_recv()
-            rows = pl.ds(group * group_rows, group_rows)
-            block = routed.at[me_t, rows]
-            for step in range(1, lines):
-                crossings[group, step] = push(
-                    block, block, cross_sem, (group, step - 1),
-                    {"tp": line_at(step) * 2 + core},
-                )
-            forwards[group] = push(block, block, fwd_sem, (group,), {"tp": partner})
-
-        def relay(group):
-            rows = pl.ds(group * group_rows, group_rows)
-            for step in range(1, lines):
-                crossings[group, step].wait_recv()
-                block = routed.at[line_at(lines - step) * 2 + core, rows]
-                relays[group, step] = push(
-                    block, block, relay_sem, (group, step - 1), {"tp": partner}
-                )
-
-        def settle(group):
-            forwards[group].wait_recv()
-            for step in range(1, lines):
-                relays[group, step].wait_recv()
-
-        def expand(half):
-            rows = pl.ds(half * half_rows, half_rows)
-
-            def one_tile(index, carry):
-                cols = pl.ds(pl.multiple_of(index * tile, tile), tile)
-                gate_sum = jnp.zeros((half_rows, tile), f32)
-                up_sum = jnp.zeros((half_rows, tile), f32)
+        first_rows = pl.ds(pl.multiple_of(me_m * capacity, capacity), capacity)
+        routed[0][me_t, first_rows] = spread_rows[:capacity]
+        square = [(turn, step) for turn in range(EXP_GROUP) for step in range(lines)]
+        square.sort(key=lambda pair: -(pair[0] + 1) // 2 - min(pair[1], lines - pair[1]))
+        square.remove((0, 0))
+
+        def chunk_rows(index, owner):
+            count = sets[index] * capacity
+            return pl.ds(pl.multiple_of(owner * count, count), count)
+
+        crossings = {
+            step: push(
+                outgoing.at[pl.ds(step * capacity, capacity)],
+                routed[1].at[
+                    me_t,
+                    pl.ds(
+                        pl.multiple_of((me_m * sets[1] + step - 1) * capacity, capacity), capacity
+                    ),
+                ],
+                cross_sem, (step - 1,), group_device(step),
+            )
+            for step in range(1, groups)
+        }
+        arrivals, mirrored = {}, {}
+
+        def spread(index):
+            rows = chunk_rows(index, me_m)
+            source = outgoing.at[pl.ds(0, capacity)] if index == 0 else routed[1].at[me_t, rows]
+            for turn, step in square:
+                arrivals[index, turn, step] = push(
+                    source, routed[index].at[me_t, rows], spread_sem[index], (turn, step),
+                    square_device(turn, step),
+                )
+            mirrored[index, 0, 0] = push(
+                source, routed[index].at[me_t, rows], mirror_sem[index], (0, 0), {"tp": partner}
+            )
+
+        def mirror(index):
+            for turn, step in square:
+                arrivals[index, turn, step].wait_recv()
+                block = routed[index].at[
+                    line_before(step) * 2 + core, chunk_rows(index, member(turn))
+                ]
+                mirrored[index, turn, step] = push(
+                    block, block, mirror_sem[index], (turn, step), {"tp": partner}
+                )
+
+        def settle(index):
+            for turn, step in [(0, 0)] + square:
+                mirrored[index, turn, step].wait_recv()
+
+        def expand(index):
+            base = sum(set_rows[:index])
+            rows = set_rows[index]
+
+            def one_tile(number, carry):
+                cols = pl.ds(pl.multiple_of(number * tile, tile), tile)
+                gate_sum = jnp.zeros((rows, tile), f32)
+                up_sum = jnp.zeros((rows, tile), f32)
                 for shard in range(shards):
-                    block = routed[shard, rows]
+                    block = routed[index][shard]
                     deep = pl.ds(shard * width, width)
                     gate_sum += jnp.dot(block, gate_v[deep, cols], preferred_element_type=f32)
                     up_sum += jnp.dot(block, up_v[deep, cols], preferred_element_type=f32)
-                hidden[rows, cols] = (
+                hidden[pl.ds(base, rows), cols] = (
                     gate_sum / (1.0 + jnp.exp(-gate_sum)) * up_sum
                 ).astype(bf16)
                 return carry
 
             lax.fori_loop(0, hidden_units // tile, one_tile, 0)
 
-        def down(half, shard):
-            return jnp.dot(
-                hidden[pl.ds(half * half_rows, half_rows)],
+        def down(index, shard):
+            base = sum(set_rows[:index])
+            return scale_ref[pl.ds(base, set_rows[index]), 0:1] * jnp.dot(
+                hidden[pl.ds(base, set_rows[index])],
                 down_v[:, pl.ds(pl.multiple_of(shard * width, width), width)],
                 preferred_element_type=f32,
             )
 
-        parts, sums = {}, {}
-
-        def shrink(half):
-            for step in list(range(1, lines)) + [0]:
-                part_send[half, step] = down(half, line_at(step) * 2 + 1 - core).astype(bf16)
-                parts[half, step] = push(
-                    part_send.at[half, step], part_pair.at[half, step], part_sem, (half, step),
+        parts, returns = {}, {}
+        line_order = list(range(1, lines)) + [0]
+
+        def shrink(index):
+            for step in line_order:
+                part_send[index][step] = down(index, line_at(step) * 2 + 1 - core).astype(bf16)
+                parts[index, step] = push(
+                    part_send[index].at[step], part_recv[index].at[step], part_sem[index], (step,),
                     {"tp": partner},
                 )
-            for step in range(1, lines):
-                other_sum[half, step - 1] = down(half, line_at(step) * 2 + core)
-            own_sum[half] = down(half, me_t)
-
-        def join(half):
-            for step in range(1, lines):
-                parts[half, step].wait_recv()
-                sum_send[half, step - 1] = (
-                    other_sum[half, step - 1] + part_pair[half, step].astype(f32)
-                ).astype(bf16)
-                sums[half, step] = push(
-                    sum_send.at[half, step - 1], sum_recv.at[half, step - 1], sum_sem,
-                    (half, step - 1), {"tp": line_at(step) * 2 + core},
-                )
-
-        backs = {}
-
-        def finish(half):
-            parts[half, 0].wait_recv()
-            value = own_sum[half] + part_pair[half, 0].astype(f32)
-            for step in range(1, lines):
-                sums[half, step].wait_recv()
-                value = value + sum_recv[half, step - 1].astype(f32)
-            value = value.astype(bf16)
-            result[pl.ds(half * half_rows, half_rows)] = value
-            first = half * (experts // halves)
-            if half == 0:
-                returned[pl.ds(0, capacity)] = value[:capacity]
-            for step in range(max(first, 1), first + experts // halves):
-                rows = pl.ds(step * capacity, capacity)
-                backs[step] = push(
-                    result.at[rows], returned.at[rows], back_sem, (step,),
-                    {"sp": lax.rem(me_s + experts - step, experts)},
-                )
-
-        forward(0)
-        forward(1)
-        relay(0)
+            for step in line_order:
+                own = down(index, line_at(step) * 2 + core)
+                parts[index, step].wait_recv()
+                own = own + part_recv[index][step].astype(f32)
+                give[index][step] = own.astype(bf16)
+                for turn in (3, 2, 1, 0):
+                    if turn == 0 and step == 0:
+                        continue
+                    returns[index, turn, step] = push(
+                        give[index].at[step, chunk_rows(index, member(turn))],
+                        take[index].at[turn, step], return_sem[index], (turn, step),
+                        square_device(turn, step),
+                    )
+                if step == 0:
+                    kept[index][...] = own
+
+        def gather_up(index):
+            total = kept[index][chunk_rows(index, me_m)]
+            for turn, step in square:
+                returns[index, turn, step].wait_recv()
+                total = total + take[index][turn, step].astype(f32)
+            return total
+
+        with scope("weights_in"):
+            for step in range(1, experts):
+                shares[step].wait_recv()
+        shared = [
+            weight_recv[lax.rem(me_g - step + groups, groups) * EXP_GROUP + owner, 0:1]
+            for step in range(groups)
+            for owner in range(EXP_GROUP)
+        ]
+        shared.append(jnp.zeros((128 - experts, token_count), f32))
+        shared = jnp.concatenate(shared, 0).T
+        base = 0
+        for index in range(len(sets)):
+            for owner in range(EXP_GROUP):
+                for step in [0] if index == 0 else range(1, groups):
+                    column = step * EXP_GROUP + owner
+                    scale_ref[pl.ds(base, capacity)] = jnp.broadcast_to(
+                        shared[step * capacity : (step + 1) * capacity, column : column + 1],
+                        (capacity, 128),
+                    )
+                    base += capacity
+        with scope("spread0"):
+            spread(0)
+        if groups > 1:
+            with scope("cross"):
+                for step in range(1, groups):
+                    crossings[step].wait_recv()
+            spread(1)
+        with scope("mirror0"):
+            mirror(0)
         for load in loads[5:7]:
             load.wait()
-        settle(0)
-        expand(0)
-        forward(2)
-        relay(1)
+        with scope("settle0"):
+            settle(0)
+        with scope("expand0"):
+            expand(0)
         loads[7].wait()
-        shrink(0)
-        forward(3)
-        settle(1)
-        join(0)
-        expand(1)
-        relay(2)
-        shrink(1)
-        settle(2)
-        join(1)
-        finish(0)
-        expand(2)
-        relay(3)
-        shrink(2)
-        settle(3)
-        join(2)
-        finish(1)
-        expand(3)
-        shrink(3)
-        join(3)
-        finish(2)
-        finish(3)
-        slot_index = lax.broadcasted_iota(jnp.int32, (token_count, row_total), 1)
-        choose = [
-            jnp.where(slot_index == at[k], 1.0, 0.0).astype(bf16)
-            for k in range(TOPK)
-        ]
-        for step in range(1, experts):
-            backs[step].wait_recv()
-        second_sum = residual_scale * normed.astype(f32)
-        back_rows = returned[...]
-        for k in range(TOPK):
-            second_sum = second_sum + routing[:, k : k + 1] * jnp.dot(
-                choose[k], back_rows, preferred_element_type=f32
-            )
-        out_ref[...] = normalize(second_sum, last_gain_ref[...], 1).astype(bf16)
+        with scope("shrink0"):
+            shrink(0)
+        returned = []
+        if groups > 1:
+            with scope("mirror1"):
+                mirror(1)
+            with scope("settle1"):
+                settle(1)
+            with scope("expand1"):
+                expand(1)
+            with scope("shrink1"):
+                shrink(1)
+            with scope("gather0"):
+                first = gather_up(0)
+            with scope("gather1"):
+                home[...] = gather_up(1).astype(bf16)
+            backs = {
+                step: push(
+                    home.at[pl.ds((step - 1) * capacity, capacity)], returned_ref.at[step - 1],
+                    back_sem, (step - 1,), group_device(-step),
+                )
+                for step in range(1, groups)
+            }
+            with scope("back"):
+                for step in range(1, groups):
+                    backs[step].wait_recv()
+                    returned.append(returned_ref[step - 1].astype(f32))
+        else:
+            first = gather_up(0)
+        second_sum = residual_scale * spread_rows.astype(f32) + jnp.concatenate([first] + returned, 0)
+        with scope("norm2"):
+            result_rows = normalize(second_sum, last_gain_ref[...], 1).astype(bf16)
+        out_ref[...] = jnp.dot(back_ref[...], result_rows, preferred_element_type=f32).astype(bf16)
         for copy in sent:
             copy.wait_send()
 
@@ -597,25 +679,31 @@
             pltpu.VMEM((2, 8, token_count), f32),
             pltpu.VMEM((2, shards - 1, 8, token_count), f32),
             dma((2, 2, shards - 1)),
-            pltpu.VMEM((row_total, width), bf16),
-            pltpu.VMEM((shards, row_total, width), bf16),
+            pltpu.VMEM((token_count, token_count), bf16),
+            pltpu.VMEM((token_count, token_count), bf16),
+            pltpu.VMEM((experts, 8, token_count), f32),
+            pltpu.VMEM((experts, 8, token_count), f32),
             dma((2, experts)),
-            dma((2, groups)),
-            dma((2, groups, other)),
-            dma((2, groups, other)),
+            pltpu.VMEM((row_total, 128), f32),
+            pltpu.VMEM((token_count, width), bf16),
             pltpu.VMEM((row_total, hidden_units), bf16),
-            pltpu.VMEM((halves, lines, half_rows, width), bf16),
-            pltpu.VMEM((halves, lines, half_rows, width), bf16),
-            pltpu.VMEM((halves, other, half_rows, width), bf16),
-            pltpu.VMEM((halves, other, half_rows, width), bf16),
-            pltpu.VMEM((halves, half_rows, width), f32),
-            pltpu.VMEM((halves, other, half_rows, width), f32),
-            dma((2, halves, lines)),
-            dma((2, halves, other)),
-            pltpu.VMEM((row_total, width), bf16),
-            pltpu.VMEM((row_total, width), bf16),
-            dma((2, experts)),
-        ],
+            dma((2, max(groups - 1, 1))),
+            pltpu.VMEM((sets[-1] * capacity, width), bf16),
+            pltpu.VMEM((max(groups - 1, 1), capacity, width), bf16),
+            dma((2, max(groups - 1, 1))),
+        ]
+        + [pltpu.VMEM((shards, rows, width), bf16) for rows in set_rows]
+        + [dma((2, EXP_GROUP, lines))] * len(sets)
+        + [dma((2, EXP_GROUP, lines))] * len(sets)
+        + [pltpu.VMEM((lines, rows, width), bf16) for rows in set_rows]
+        + [pltpu.VMEM((lines, rows, width), bf16) for rows in set_rows]
+        + [dma((2, lines))] * len(sets)
+        + [pltpu.VMEM((lines, rows, width), bf16) for rows in set_rows]
+        + [
+            pltpu.VMEM((EXP_GROUP, lines, blocks * capacity, width), bf16) for blocks in sets
+        ]
+        + [dma((2, EXP_GROUP, lines))] * len(sets)
+        + [pltpu.VMEM((rows, width), f32) for rows in set_rows],
         compiler_params=pltpu.CompilerParams(
             collective_id=0, has_side_effects=True, vmem_limit_bytes=58 << 20
         ),

time: 82.3 us -> 75.2 us (0.914)
  Pallas kernels: 80.6 us -> 73.5 us
    pallas_call x1, Pallas kernels: 80.6 us -> 73.5 us  [layer(): pl.pallas_call(kernel, out_shape=jax.ShapeDtypeStruct((token_count, width...]
where the time goes in v2:
time: 75.2 us; the launch traced here: 75.1 us
  Pallas kernels  73.5 us (98%)
  local copies, waits for them, and re-layouts  1.57 us (2%)
    pallas_call x1, Pallas kernels, layer(): pl.pallas_call(kernel, out_shape=jax.ShapeDtypeStruct((token_count, width...  73.5 us
    unnamed x1, local copies, waits for them, and re-layouts  1.57 us

profile of v2, /device:TPU:0, one launch (start us, length us, event | category | flops | bytes accessed | tf_op | source)
XLA Modules:
  0.0 75.1 jit_solution(973897132044004451)
XLA Ops:
  0.0 73.5 %shard_map.154 = bf16[128,512]{1,0:T(8,128)(2,1)} custom-call(f32[2,16,128]{2,1,0:T(8,128)} %constant.4.clone.row_hbm, f32[2,64,128]{2,1,0:T(8,128)} %constant.5.clone.column_hbm, f32[1,64]{1,0:T(1,128)} %bitcast.10, f32[1,64]{1,0:T(1,128)} %bitcast.11, f32[1,512]{1,0:T(1,128)} %bitcast.6, s32[2,128]{1,0:T(2,128)} %bitcast.8, f32[2,128]{1,0:T(2,128)} %bitcast.9, ...), custom_call_target="tpu_custom_call" | custom-call | tf_op jit(solution)/shard_map/pallas_call | solution.py:641
  73.5 1.6 %copy.18 = bf16[128,512]{1,0:T(8,128)(2,1)} copy(bf16[128,512]{1,0:T(8,128)(2,1)} %shard_map.154) | data formatting | bytes 262144

commit v3 on v2

--- a/solution.py
+++ b/solution.py
@@ -80,13 +80,19 @@
     query_rows = 2 * token_count
     ring_minor = 1 << ((experts.bit_length() - 1) // 2)
     ring_half = experts // 2
-    pieces = 4
+    pieces = 8
     piece = token_count // pieces
     lines = shards // 2
     groups = experts // EXP_GROUP
     capacity = token_count // groups
-    sets = (1, groups - 1) if groups > 1 else (1,)
-    set_rows = [EXP_GROUP * blocks * capacity for blocks in sets]
+    splits = 2 if capacity % 32 == 0 else 1
+    stretch = capacity // splits
+    sets = [([0], part) for part in range(splits)]
+    if groups > 1:
+        sets += [(list(range(1, groups)), part) for part in range(splits)]
+    away_sets = range(splits, len(sets))
+    member_rows = [len(steps) * stretch for steps, _ in sets]
+    set_rows = [EXP_GROUP * rows for rows in member_rows]
     row_total = sum(set_rows)
     hidden_units = gate_weight.shape[2]
     tile = min(256, hidden_units)
@@ -98,17 +104,17 @@
         q_hbm, k_hbm, v_hbm, res_hbm, ow_hbm, gate_hbm, up_hbm, down_hbm, out_ref,
         row_ref, column_ref, q_gain_ref, k_gain_ref, gain_ref, ids_ref, rw_ref, last_gain_ref,
         small_sem, q_v, k_v, v_v, res_ref, ow_ref, gate_v, up_v, down_v, weight_sem,
-        ring_ref, ring_send, ring_recv, q_pad, flash_out, flash_max, flash_sum, att_ref,
+        send_sem, ring_ref, ring_recv, q_pad, flash_out, flash_max, flash_sum, att_ref,
         mix_send, mix_pair, line_send, line_recv, mix_sem, line_sem,
         stat_send, stat_recv, stat_sem,
         perm_ref, back_ref, weight_send, weight_recv, share_sem, scale_ref, outgoing, hidden,
-        cross_sem, home, returned_ref, back_sem, *per_set,
+        cross_sem, spread_sem, mirror_sem, part_sem, return_sem, home, returned_ref, back_sem,
+        *per_set,
     ):
         count = len(sets)
-        (
-            routed, spread_sem, mirror_sem, part_send, part_recv, part_sem, give, take, return_sem,
-            kept,
-        ) = [per_set[i * count : (i + 1) * count] for i in range(10)]
+        routed, part_send, part_recv, give, take, kept = [
+            per_set[i * count : (i + 1) * count] for i in range(6)
+        ]
         me_s = lax.axis_index("sp")
         me_t = lax.axis_index("tp")
         line = me_t // 2
@@ -175,19 +181,29 @@
                 )
             )
         ]
-        for load in loads[:3] + small_loads + loads[3:]:
+        for load in loads[:3] + small_loads:
             load.start()
-        sent = []
-
-        def push(source, target, sems, index, device):
+        sent_bytes = dict.fromkeys(range(8), 0)
+
+        def push(source, target, phase, recv_sem, device):
             copy = pltpu.make_async_remote_copy(
-                src_ref=source, dst_ref=target,
-                send_sem=sems.at[(0,) + index], recv_sem=sems.at[(1,) + index],
+                src_ref=source, dst_ref=target, send_sem=send_sem.at[phase], recv_sem=recv_sem,
                 device_id=device, device_id_type=MESH,
             )
             copy.start()
-            sent.append(copy)
+            sent_bytes[phase] += int(np.prod(source.shape)) * jnp.dtype(source.dtype).itemsize
             return copy
+
+        def stretch_of(size):
+            rows = size // (2 * hidden_units)
+            assert rows * 2 * hidden_units == size and rows % 8 == 0 and rows <= feature_total
+            return gate_v.at[pl.ds(0, rows)]
+
+        def waiter(region, sems):
+            return pltpu.make_async_remote_copy(
+                src_ref=region, dst_ref=region, send_sem=sems, recv_sem=sems,
+                device_id={"tp": partner}, device_id_type=MESH,
+            )
 
         lane_pair = lax.broadcasted_iota(jnp.int32, (token_count, pair_width), 1)
         low_half = lane_pair < HEAD_DIM
@@ -200,6 +216,10 @@
         ).astype(bf16)
         for load in small_loads:
             load.wait()
+        for load in loads[:3]:
+            load.wait()
+        for load in loads[3:]:
+            load.start()
 
         def rotary(part):
             blocks = []
@@ -231,8 +251,6 @@
         def swap(rows):
             return pltpu.roll(rows, HEAD_DIM, 1)
 
-        loads[0].wait()
-        loads[1].wait()
         for pair in range((key_heads + 1) // 2):
             if key_heads == 1:
                 key_pair = jnp.concatenate([k_v[...]] * 2, 1).astype(f32)
@@ -266,14 +284,10 @@
                 span = pl.ds(part * piece, piece)
                 source_slot = (hop - 1) if way == 0 else (experts - hop + 1) % experts
                 target_slot = hop if way == 0 else experts - hop
-                copy = pltpu.make_async_remote_copy(
-                    src_ref=ring_ref.at[source_slot, span], dst_ref=ring_ref.at[target_slot, span],
-                    send_sem=ring_send.at[way, hop - 1, part],
-                    recv_sem=ring_recv.at[way, hop - 1, part],
-                    device_id={"sp": right if way == 0 else left}, device_id_type=MESH,
-                )
-                copy.start()
-                sent.append(copy)
+                copy = push(
+                    ring_ref.at[source_slot, span], ring_ref.at[target_slot, span], 0,
+                    ring_recv.at[way, hop - 1, part], {"sp": right if way == 0 else left},
+                )
                 ring[way, hop, part] = copy
 
         def attend(slot, head, first):
@@ -345,21 +359,18 @@
                     by_slot[expert : expert + 1], (8, token_count)
                 )
             weight_recv[me_s] = weight_send[me_s]
-            return {
-                step: push(
-                    weight_send.at[lax.rem(me_s + step, experts)], weight_recv.at[me_s], share_sem,
-                    (step,), {"sp": lax.rem(me_s + step, experts)},
-                )
-                for step in range(1, experts)
-            }
+            for step in range(1, experts):
+                push(
+                    weight_send.at[lax.rem(me_s + step, experts)], weight_recv.at[me_s], 1,
+                    share_sem, {"sp": lax.rem(me_s + step, experts)},
+                )
 
         waiting = []
         for part in range(pieces):
             pass_on(1, part)
-        loads[2].wait()
         for head in range(key_heads):
             prepare(head)
-        shares = route()
+        route()
         waiting += [(0, head, True) for head in range(key_heads)]
         for hop in range(2, ring_half + 1):
             for part in range(pieces):
@@ -384,6 +395,7 @@
                         ring[way, ring_half, part].wait_recv()
         for head in range(key_heads):
             attend(ring_half, head, False)
+        for head in range(key_heads):
             result_rows = flash_out[head] / flash_sum[head]
             att_ref[:, pl.ds(head * pair_width, pair_width)] = (
                 jnp.concatenate([result_rows[:, :token_count], result_rows[:, token_count:]], 0)
@@ -406,7 +418,7 @@
         pair = {}
         for step in list(range(1, lines)) + [0]:
             pair[step] = push(
-                mix_send.at[step], mix_pair.at[step], mix_sem, (step,), {"tp": partner}
+                mix_send.at[step], mix_pair.at[step], 2, mix_sem.at[step], {"tp": partner}
             )
         across = {}
         for step in range(1, lines):
@@ -414,7 +426,7 @@
             pair[step].wait_recv()
             line_send[step - 1] = (mine + mix_pair[step].astype(f32)).astype(bf16)
             across[step] = push(
-                line_send.at[step - 1], line_recv.at[step - 1], line_sem, (step - 1,),
+                line_send.at[step - 1], line_recv.at[step - 1], 2, line_sem.at[step - 1],
                 {"tp": line_at(step) * 2 + core},
             )
         total = mix(me_t)
@@ -431,15 +443,13 @@
             squares = jnp.sum(values * values, 1, keepdims=True)
             both = jnp.where(lane == 0, sums, jnp.where(lane == 1, squares, 0.0)).T[:8]
             stat_send[turn] = both
-            stats = [
+            for step in range(1, shards):
                 push(
-                    stat_send.at[turn], stat_recv.at[turn, step - 1], stat_sem,
-                    (turn, step - 1), {"tp": lax.rem(me_t + step, shards)},
-                )
-                for step in range(1, shards)
-            ]
+                    stat_send.at[turn], stat_recv.at[turn, step - 1], 3, stat_sem.at[turn],
+                    {"tp": lax.rem(me_t + step, shards)},
+                )
+            waiter(stat_recv.at[turn], stat_sem.at[turn]).wait_recv()
             for step in range(1, shards):
-                stats[step - 1].wait_recv()
                 both = both + stat_recv[turn, step - 1]
             columns = jnp.concatenate([both] * 16, 0).T
             center = columns[:, 0:1] / feature_total
@@ -450,56 +460,62 @@
             normed = normalize(total, gain_ref[...], 0).astype(bf16)
         spread_rows = jnp.dot(perm_ref[...], normed, preferred_element_type=f32).astype(bf16)
         outgoing[...] = spread_rows
-        first_rows = pl.ds(pl.multiple_of(me_m * capacity, capacity), capacity)
-        routed[0][me_t, first_rows] = spread_rows[:capacity]
         square = [(turn, step) for turn in range(EXP_GROUP) for step in range(lines)]
         square.sort(key=lambda pair: -(pair[0] + 1) // 2 - min(pair[1], lines - pair[1]))
         square.remove((0, 0))
 
-        def chunk_rows(index, owner):
-            count = sets[index] * capacity
+        def member_span(index, owner):
+            count = member_rows[index]
             return pl.ds(pl.multiple_of(owner * count, count), count)
 
-        crossings = {
-            step: push(
-                outgoing.at[pl.ds(step * capacity, capacity)],
-                routed[1].at[
-                    me_t,
-                    pl.ds(
-                        pl.multiple_of((me_m * sets[1] + step - 1) * capacity, capacity), capacity
-                    ),
-                ],
-                cross_sem, (step - 1,), group_device(step),
-            )
-            for step in range(1, groups)
-        }
-        arrivals, mirrored = {}, {}
+        crossings = {}
+        for index in away_sets:
+            for place, step in enumerate(sets[index][0]):
+                crossings[index, step] = push(
+                    outgoing.at[pl.ds(step * capacity + sets[index][1] * stretch, stretch)],
+                    routed[index].at[
+                        me_t,
+                        pl.ds(
+                            pl.multiple_of(
+                                me_m * member_rows[index] + place * stretch, stretch
+                            ),
+                            stretch,
+                        ),
+                    ],
+                    4, cross_sem.at[index - splits, place], group_device(step),
+                )
+        arrivals = {}
 
         def spread(index):
-            rows = chunk_rows(index, me_m)
-            source = outgoing.at[pl.ds(0, capacity)] if index == 0 else routed[1].at[me_t, rows]
+            rows = member_span(index, me_m)
+            if index < splits:
+                span = slice(index * stretch, (index + 1) * stretch)
+                routed[index][me_t, rows] = spread_rows[span]
+                source = outgoing.at[pl.ds(index * stretch, stretch)]
+            else:
+                for step in sets[index][0]:
+                    crossings[index, step].wait_recv()
+                source = routed[index].at[me_t, rows]
             for turn, step in square:
                 arrivals[index, turn, step] = push(
-                    source, routed[index].at[me_t, rows], spread_sem[index], (turn, step),
+                    source, routed[index].at[me_t, rows], 4, spread_sem.at[index, turn, step],
                     square_device(turn, step),
                 )
-            mirrored[index, 0, 0] = push(
-                source, routed[index].at[me_t, rows], mirror_sem[index], (0, 0), {"tp": partner}
+            push(
+                source, routed[index].at[me_t, rows], 5, mirror_sem.at[index], {"tp": partner}
             )
 
         def mirror(index):
             for turn, step in square:
                 arrivals[index, turn, step].wait_recv()
                 block = routed[index].at[
-                    line_before(step) * 2 + core, chunk_rows(index, member(turn))
+                    line_before(step) * 2 + core, member_span(index, member(turn))
                 ]
-                mirrored[index, turn, step] = push(
-                    block, block, mirror_sem[index], (turn, step), {"tp": partner}
-                )
+                push(block, block, 5, mirror_sem.at[index], {"tp": partner})
 
         def settle(index):
-            for turn, step in [(0, 0)] + square:
-                mirrored[index, turn, step].wait_recv()
+            size = lines * set_rows[index] * width * 2
+            waiter(stretch_of(size), mirror_sem.at[index]).wait_recv()
 
         def expand(index):
             base = sum(set_rows[:index])
@@ -529,15 +545,15 @@
                 preferred_element_type=f32,
             )
 
-        parts, returns = {}, {}
+        parts = {}
         line_order = list(range(1, lines)) + [0]
 
         def shrink(index):
             for step in line_order:
                 part_send[index][step] = down(index, line_at(step) * 2 + 1 - core).astype(bf16)
                 parts[index, step] = push(
-                    part_send[index].at[step], part_recv[index].at[step], part_sem[index], (step,),
-                    {"tp": partner},
+                    part_send[index].at[step], part_recv[index].at[step], 6,
+                    part_sem.at[index, step], {"tp": partner},
                 )
             for step in line_order:
                 own = down(index, line_at(step) * 2 + core)
@@ -547,24 +563,26 @@
                 for turn in (3, 2, 1, 0):
                     if turn == 0 and step == 0:
                         continue
-                    returns[index, turn, step] = push(
-                        give[index].at[step, chunk_rows(index, member(turn))],
-                        take[index].at[turn, step], return_sem[index], (turn, step),
+                    push(
+                        give[index].at[step, member_span(index, member(turn))],
+                        take[index].at[turn, step], 7, return_sem.at[index],
                         square_device(turn, step),
                     )
                 if step == 0:
                     kept[index][...] = own
 
         def gather_up(index):
-            total = kept[index][chunk_rows(index, me_m)]
+            total = kept[index][member_span(index, me_m)]
+            size = len(square) * member_rows[index] * width * 2
+            waiter(stretch_of(size), return_sem.at[index]).wait_recv()
             for turn, step in square:
-                returns[index, turn, step].wait_recv()
                 total = total + take[index][turn, step].astype(f32)
             return total
 
+        for index in range(splits):
+            spread(index)
         with scope("weights_in"):
-            for step in range(1, experts):
-                shares[step].wait_recv()
+            waiter(weight_recv.at[pl.ds(0, experts - 1)], share_sem).wait_recv()
         shared = [
             weight_recv[lax.rem(me_g - step + groups, groups) * EXP_GROUP + owner, 0:1]
             for step in range(groups)
@@ -573,66 +591,64 @@
         shared.append(jnp.zeros((128 - experts, token_count), f32))
         shared = jnp.concatenate(shared, 0).T
         base = 0
-        for index in range(len(sets)):
+        for steps, part in sets:
             for owner in range(EXP_GROUP):
-                for step in [0] if index == 0 else range(1, groups):
+                for step in steps:
                     column = step * EXP_GROUP + owner
-                    scale_ref[pl.ds(base, capacity)] = jnp.broadcast_to(
-                        shared[step * capacity : (step + 1) * capacity, column : column + 1],
-                        (capacity, 128),
+                    top = step * capacity + part * stretch
+                    scale_ref[pl.ds(base, stretch)] = jnp.broadcast_to(
+                        shared[top : top + stretch, column : column + 1], (stretch, 128)
                     )
-                    base += capacity
-        with scope("spread0"):
-            spread(0)
-        if groups > 1:
-            with scope("cross"):
-                for step in range(1, groups):
-                    crossings[step].wait_recv()
-            spread(1)
+                    base += stretch
+        for index in away_sets:
+            with scope(f"cross{index}"):
+                spread(index)
         with scope("mirror0"):
             mirror(0)
-        for load in loads[5:7]:
-            load.wait()
-        with scope("settle0"):
-            settle(0)
-        with scope("expand0"):
-            expand(0)
-        loads[7].wait()
-        with scope("shrink0"):
-            shrink(0)
-        returned = []
-        if groups > 1:
-            with scope("mirror1"):
-                mirror(1)
-            with scope("settle1"):
-                settle(1)
-            with scope("expand1"):
-                expand(1)
-            with scope("shrink1"):
-                shrink(1)
-            with scope("gather0"):
-                first = gather_up(0)
-            with scope("gather1"):
-                home[...] = gather_up(1).astype(bf16)
-            backs = {
-                step: push(
-                    home.at[pl.ds((step - 1) * capacity, capacity)], returned_ref.at[step - 1],
-                    back_sem, (step - 1,), group_device(-step),
-                )
-                for step in range(1, groups)
-            }
-            with scope("back"):
-                for step in range(1, groups):
-                    backs[step].wait_recv()
-                    returned.append(returned_ref[step - 1].astype(f32))
-        else:
-            first = gather_up(0)
-        second_sum = residual_scale * spread_rows.astype(f32) + jnp.concatenate([first] + returned, 0)
+        with scope("weights"):
+            for load in loads[5:]:
+                load.wait()
+        for index in range(len(sets)):
+            with scope(f"settle{index}"):
+                settle(index)
+            with scope(f"expand{index}"):
+                expand(index)
+            if index + 1 < len(sets):
+                with scope(f"mirror{index + 1}"):
+                    mirror(index + 1)
+            with scope(f"shrink{index}"):
+                shrink(index)
+        with scope("gatherA"):
+            combined = [gather_up(index) for index in range(splits)]
+        backs = {}
+        for index in away_sets:
+            with scope(f"gather{index}"):
+                home[index - splits] = gather_up(index).astype(bf16)
+            for place, step in enumerate(sets[index][0]):
+                backs[step, sets[index][1]] = push(
+                    home.at[index - splits, pl.ds(place * stretch, stretch)],
+                    returned_ref.at[step - 1, pl.ds(sets[index][1] * stretch, stretch)],
+                    7, back_sem.at[index - splits, place], group_device(-step),
+                )
+        with scope("back"):
+            for step in range(1, groups):
+                for part in range(splits):
+                    backs[step, part].wait_recv()
+                combined.append(returned_ref[step - 1].astype(f32))
+        second_sum = residual_scale * spread_rows.astype(f32) + jnp.concatenate(combined, 0)
         with scope("norm2"):
             result_rows = normalize(second_sum, last_gain_ref[...], 1).astype(bf16)
         out_ref[...] = jnp.dot(back_ref[...], result_rows, preferred_element_type=f32).astype(bf16)
-        for copy in sent:
-            copy.wait_send()
+        with scope("sendwait"):
+            regions = {
+                0: ring_ref.at[pl.ds(1, experts - 1)], 1: weight_recv.at[pl.ds(1, experts - 1)],
+                3: stat_recv,
+            }
+            for phase in range(8):
+                region = regions[phase] if phase in regions else stretch_of(sent_bytes[phase])
+                size = int(np.prod(region.shape)) * jnp.dtype(region.dtype).itemsize
+                assert size == sent_bytes[phase]
+                waiter(region, send_sem.at[phase]).wait_send()
 
     vmem = pl.BlockSpec(memory_space=pltpu.VMEM)
     hbm = pl.BlockSpec(memory_space=pltpu.HBM)
@@ -640,7 +656,7 @@
     other = max(lines - 1, 1)
     return pl.pallas_call(
         kernel,
-        out_shape=jax.ShapeDtypeStruct((token_count, width), bf16),
+        out_shape=pltpu.VMEM((token_count, width), bf16),
         in_specs=[hbm] * 16,
         out_specs=vmem,
         scratch_shapes=[
@@ -662,8 +678,8 @@
             pltpu.VMEM(up_weight.shape[1:], bf16),
             pltpu.VMEM(down_weight.shape[1:], bf16),
             dma((8,)),
+            dma((8,)),
             pltpu.VMEM((experts, token_count, key_heads * pair_width), bf16),
-            dma((2, ring_half, pieces)),
             dma((2, ring_half, pieces)),
             pltpu.VMEM((key_heads, query_rows, pair_width), bf16),
             pltpu.VMEM((key_heads, HEAD_DIM, query_rows), f32),
@@ -674,44 +690,45 @@
             pltpu.VMEM((lines, token_count, width), bf16),
             pltpu.VMEM((other, token_count, width), bf16),
             pltpu.VMEM((other, token_count, width), bf16),
-            dma((2, lines)),
-            dma((2, other)),
+            dma((lines,)),
+            dma((other,)),
             pltpu.VMEM((2, 8, token_count), f32),
             pltpu.VMEM((2, shards - 1, 8, token_count), f32),
-            dma((2, 2, shards - 1)),
+            dma((2,)),
             pltpu.VMEM((token_count, token_count), bf16),
             pltpu.VMEM((token_count, token_count), bf16),
             pltpu.VMEM((experts, 8, token_count), f32),
             pltpu.VMEM((experts, 8, token_count), f32),
-            dma((2, experts)),
+            dma,
             pltpu.VMEM((row_total, 128), f32),
             pltpu.VMEM((token_count, width), bf16),
             pltpu.VMEM((row_total, hidden_units), bf16),
-            dma((2, max(groups - 1, 1))),
-            pltpu.VMEM((sets[-1] * capacity, width), bf16),
+            dma((splits, max(groups - 1, 1))),
+            dma((len(sets), EXP_GROUP, lines)),
+            dma((len(sets),)),
+            dma((len(sets), lines)),
+            dma((len(sets),)),
+            pltpu.VMEM((splits, member_rows[-1], width), bf16),
             pltpu.VMEM((max(groups - 1, 1), capacity, width), bf16),
-            dma((2, max(groups - 1, 1))),
+            dma((splits, max(groups - 1, 1))),
         ]
         + [pltpu.VMEM((shards, rows, width), bf16) for rows in set_rows]
-        + [dma((2, EXP_GROUP, lines))] * len(sets)
-        + [dma((2, EXP_GROUP, lines))] * len(sets)
-        + [pltpu.VMEM((lines, rows, width), bf16) for rows in set_rows]
-        + [pltpu.VMEM((lines, rows, width), bf16) for rows in set_rows]
-        + [dma((2, lines))] * len(sets)
-        + [pltpu.VMEM((lines, rows, width), bf16) for rows in set_rows]
-        + [
-            pltpu.VMEM((EXP_GROUP, lines, blocks * capacity, width), bf16) for blocks in sets
-        ]
-        + [dma((2, EXP_GROUP, lines))] * len(sets)
+        + [pltpu.VMEM((lines, rows, width), bf16) for rows in set_rows] * 3
+        + [pltpu.VMEM((EXP_GROUP, lines, rows, width), bf16) for rows in member_rows]
         + [pltpu.VMEM((rows, width), f32) for rows in set_rows],
         compiler_params=pltpu.CompilerParams(
-            collective_id=0, has_side_effects=True, vmem_limit_bytes=58 << 20
+            collective_id=0, has_side_effects=True, vmem_limit_bytes=48 << 20
         ),
     )(
-        row_table, column_table, query_gain.reshape(1, -1), key_gain.reshape(1, -1),
-        norm_gain.reshape(1, -1), expert_ids.T, route_weights.T,
-        final_gain.reshape(1, -1), queries, key_rows, value_rows, residual, out_weight,
-        gate_weight, up_weight, down_weight,
+        *(
+            pltpu.with_memory_space_constraint(array, pltpu.HBM)
+            for array in (
+                jnp.asarray(row_table), jnp.asarray(column_table), query_gain.reshape(1, -1),
+                key_gain.reshape(1, -1), norm_gain.reshape(1, -1), expert_ids.T, route_weights.T,
+                final_gain.reshape(1, -1), queries, key_rows, value_rows, residual, out_weight,
+                gate_weight, up_weight, down_weight,
+            )
+        )
     )
 
 

time: 75.2 us -> 67.6 us (0.90)
  Pallas kernels: 73.5 us -> 66.7 us
  local copies, waits for them, and re-layouts: 1.57 us -> 0.66 us
    pallas_call x1, Pallas kernels: 73.5 us -> 66.7 us  [layer(): pl.pallas_call(kernel, out_shape=pltpu.VMEM((token_count, width), bf16),...]
    unnamed x1, local copies, waits for them, and re-layouts: 1.57 us -> 0.66 us
where the time goes in v3:
time: 67.6 us; the launch traced here: 67.3 us
  Pallas kernels  66.7 us (99%)
    pallas_call x1, Pallas kernels, layer(): pl.pallas_call(kernel, out_shape=pltpu.VMEM((token_count, width), bf16),...  66.7 us

profile of v3, /device:TPU:0, one launch (start us, length us, event | category | flops | bytes accessed | tf_op | source)
XLA Modules:
  0.0 67.3 jit_solution(15861820001038497614)
XLA Ops:
  0.0 66.7 %shard_map.154 = bf16[128,512]{1,0:T(8,128)(2,1)S(1)} custom-call(f32[2,16,128]{2,1,0:T(8,128)} %constant.4.clone.row_hbm, f32[2,64,128]{2,1,0:T(8,128)} %constant.5.clone.column_hbm, f32[1,64]{1,0:T(1,128)} %bitcast.10, f32[1,64]{1,0:T(1,128)} %bitcast.11, f32[1,512]{1,0:T(1,128)} %bitcast.6, s32[2,128]{1,0:T(2,128)} %bitcast.8, f32[2,128]{1,0:T(2,128)} %bitcast.9, ...), custom_call_target="tpu_custom_call" | custom-call | tf_op jit(solution)/shard_map/pallas_call | solution.py:657
  66.7 0.7 copy.18

commit v4 on v3

--- a/solution.py
+++ b/solution.py
@@ -87,10 +87,12 @@
     capacity = token_count // groups
     splits = 2 if capacity % 32 == 0 else 1
     stretch = capacity // splits
-    sets = [([0], part) for part in range(splits)]
-    if groups > 1:
-        sets += [(list(range(1, groups)), part) for part in range(splits)]
-    away_sets = range(splits, len(sets))
+    near_sets = [([0], part) for part in range(splits)]
+    far_sets = [(list(range(1, groups)), part) for part in range(splits)] if groups > 1 else []
+    sets = near_sets[:1] + far_sets + near_sets[1:]
+    home_sets = [index for index, (steps, _) in enumerate(sets) if steps == [0]]
+    away_sets = [index for index, (steps, _) in enumerate(sets) if steps != [0]]
+    far_rows = (groups - 1) * stretch if groups > 1 else stretch
     member_rows = [len(steps) * stretch for steps, _ in sets]
     set_rows = [EXP_GROUP * rows for rows in member_rows]
     row_total = sum(set_rows)
@@ -112,8 +114,8 @@
         *per_set,
     ):
         count = len(sets)
-        routed, part_send, part_recv, give, take, kept = [
-            per_set[i * count : (i + 1) * count] for i in range(6)
+        routed, part_send, part_recv, give, take, kept, own_sum = [
+            per_set[i * count : (i + 1) * count] for i in range(7)
         ]
         me_s = lax.axis_index("sp")
         me_t = lax.axis_index("tp")
@@ -411,31 +413,35 @@
                 preferred_element_type=f32,
             )
 
-        with scope("mix"):
-            pass
-        for step in range(lines):
+        across = {}
+        pair = {}
+
+        def send_pair(step):
             mix_send[step] = mix(line_at(step) * 2 + 1 - core).astype(bf16)
-        pair = {}
-        for step in list(range(1, lines)) + [0]:
             pair[step] = push(
                 mix_send.at[step], mix_pair.at[step], 2, mix_sem.at[step], {"tp": partner}
             )
-        across = {}
+
+        for step in range(1, lines):
+            send_pair(step)
         for step in range(1, lines):
             mine = mix(line_at(step) * 2 + core)
-            pair[step].wait_recv()
+            with scope("pairwait"):
+                pair[step].wait_recv()
             line_send[step - 1] = (mine + mix_pair[step].astype(f32)).astype(bf16)
             across[step] = push(
                 line_send.at[step - 1], line_recv.at[step - 1], 2, line_sem.at[step - 1],
                 {"tp": line_at(step) * 2 + core},
             )
+        send_pair(0)
         total = mix(me_t)
         pair[0].wait_recv()
         total = total + mix_pair[0].astype(f32)
         loads[4].wait()
         total = total + residual_scale * res_ref[...].astype(f32)
         for step in range(1, lines):
-            across[step].wait_recv()
+            with scope("acrosswait"):
+                across[step].wait_recv()
             total = total + line_recv[step - 1].astype(f32)
 
         def normalize(values, gain, turn):
@@ -469,7 +475,8 @@
             return pl.ds(pl.multiple_of(owner * count, count), count)
 
         crossings = {}
-        for index in away_sets:
+
+        def cross(index):
             for place, step in enumerate(sets[index][0]):
                 crossings[index, step] = push(
                     outgoing.at[pl.ds(step * capacity + sets[index][1] * stretch, stretch)],
@@ -482,16 +489,17 @@
                             stretch,
                         ),
                     ],
-                    4, cross_sem.at[index - splits, place], group_device(step),
-                )
+                    4, cross_sem.at[away_sets.index(index), place], group_device(step),
+                )
+
         arrivals = {}
 
         def spread(index):
             rows = member_span(index, me_m)
-            if index < splits:
-                span = slice(index * stretch, (index + 1) * stretch)
-                routed[index][me_t, rows] = spread_rows[span]
-                source = outgoing.at[pl.ds(index * stretch, stretch)]
+            if index in home_sets:
+                top = sets[index][1] * stretch
+                routed[index][me_t, rows] = spread_rows[top : top + stretch]
+                source = outgoing.at[pl.ds(top, stretch)]
             else:
                 for step in sets[index][0]:
                     crossings[index, step].wait_recv()
@@ -556,9 +564,12 @@
                     part_sem.at[index, step], {"tp": partner},
                 )
             for step in line_order:
-                own = down(index, line_at(step) * 2 + core)
+                own_sum[index][step] = down(index, line_at(step) * 2 + core)
+
+        def join(index):
+            for step in line_order:
                 parts[index, step].wait_recv()
-                own = own + part_recv[index][step].astype(f32)
+                own = own_sum[index][step] + part_recv[index][step].astype(f32)
                 give[index][step] = own.astype(bf16)
                 for turn in (3, 2, 1, 0):
                     if turn == 0 and step == 0:
@@ -579,8 +590,11 @@
                 total = total + take[index][turn, step].astype(f32)
             return total
 
-        for index in range(splits):
-            spread(index)
+        for index in away_sets[:1]:
+            cross(index)
+        spread(0)
+        for index in away_sets[1:]:
+            cross(index)
         with scope("weights_in"):
             waiter(weight_recv.at[pl.ds(0, experts - 1)], share_sem).wait_recv()
         shared = [
@@ -600,7 +614,7 @@
                         shared[top : top + stretch, column : column + 1], (stretch, 128)
                     )
                     base += stretch
-        for index in away_sets:
+        for index in away_sets + home_sets[1:]:
             with scope(f"cross{index}"):
                 spread(index)
         with scope("mirror0"):
@@ -616,20 +630,26 @@
             if index + 1 < len(sets):
                 with scope(f"mirror{index + 1}"):
                     mirror(index + 1)
+            if index == 1:
+                with scope("join0"):
+                    join(0)
             with scope(f"shrink{index}"):
                 shrink(index)
-        with scope("gatherA"):
-            combined = [gather_up(index) for index in range(splits)]
+            if index > 0 or len(sets) == 1:
+                with scope(f"join{index}"):
+                    join(index)
         backs = {}
-        for index in away_sets:
+        for order, index in enumerate(away_sets):
             with scope(f"gather{index}"):
-                home[index - splits] = gather_up(index).astype(bf16)
+                home[order] = gather_up(index).astype(bf16)
             for place, step in enumerate(sets[index][0]):
                 backs[step, sets[index][1]] = push(
-                    home.at[index - splits, pl.ds(place * stretch, stretch)],
+                    home.at[order, pl.ds(place * stretch, stretch)],
                     returned_ref.at[step - 1, pl.ds(sets[index][1] * stretch, stretch)],
-                    7, back_sem.at[index - splits, place], group_device(-step),
-                )
+                    7, back_sem.at[order, place], group_device(-step),
+                )
+        with scope("gatherA"):
+            combined = [gather_up(index) for index in home_sets]
         with scope("back"):
             for step in range(1, groups):
                 for part in range(splits):
@@ -708,14 +728,15 @@
             dma((len(sets),)),
             dma((len(sets), lines)),
             dma((len(sets),)),
-            pltpu.VMEM((splits, member_rows[-1], width), bf16),
+            pltpu.VMEM((splits, far_rows, width), bf16),
             pltpu.VMEM((max(groups - 1, 1), capacity, width), bf16),
             dma((splits, max(groups - 1, 1))),
         ]
         + [pltpu.VMEM((shards, rows, width), bf16) for rows in set_rows]
         + [pltpu.VMEM((lines, rows, width), bf16) for rows in set_rows] * 3
         + [pltpu.VMEM((EXP_GROUP, lines, rows, width), bf16) for rows in member_rows]
-        + [pltpu.VMEM((rows, width), f32) for rows in set_rows],
+        + [pltpu.VMEM((rows, width), f32) for rows in set_rows]
+        + [pltpu.VMEM((lines, rows, width), f32) for rows in set_rows],
         compiler_params=pltpu.CompilerParams(
             collective_id=0, has_side_effects=True, vmem_limit_bytes=48 << 20
         ),

time: 67.6 us -> 64.5 us (0.954)
  Pallas kernels: 66.7 us -> 63.6 us
    pallas_call x1, Pallas kernels: 66.7 us -> 63.6 us  [layer(): pl.pallas_call(kernel, out_shape=pltpu.VMEM((token_count, width), bf16),...]
where the time goes in v4:
time: 64.5 us; the launch traced here: 64.3 us
  Pallas kernels  63.6 us (99%)
  local copies, waits for them, and re-layouts  0.66 us (1%)
    pallas_call x1, Pallas kernels, layer(): pl.pallas_call(kernel, out_shape=pltpu.VMEM((token_count, width), bf16),...  63.6 us

profile of v4, /device:TPU:0, one launch (start us, length us, event | category | flops | bytes accessed | tf_op | source)
XLA Modules:
  0.0 64.3 jit_solution(16227000351376390754)
XLA Ops:
  0.0 63.6 %shard_map.154 = bf16[128,512]{1,0:T(8,128)(2,1)S(1)} custom-call(f32[2,16,128]{2,1,0:T(8,128)} %constant.4.clone.row_hbm, f32[2,64,128]{2,1,0:T(8,128)} %constant.5.clone.column_hbm, f32[1,64]{1,0:T(1,128)} %bitcast.10, f32[1,64]{1,0:T(1,128)} %bitcast.11, f32[1,512]{1,0:T(1,128)} %bitcast.6, s32[2,128]{1,0:T(2,128)} %bitcast.8, f32[2,128]{1,0:T(2,128)} %bitcast.9, ...), custom_call_target="tpu_custom_call" | custom-call | tf_op jit(solution)/shard_map/pallas_call | solution.py:677
  63.6 0.7 %copy.18 = bf16[128,512]{1,0:T(8,128)(2,1)} copy(bf16[128,512]{1,0:T(8,128)(2,1)S(1)} %shard_map.154) | data formatting | bytes 262144

commit v5 on v4

--- a/solution.py
+++ b/solution.py
@@ -110,7 +110,7 @@
         mix_send, mix_pair, line_send, line_recv, mix_sem, line_sem,
         stat_send, stat_recv, stat_sem,
         perm_ref, back_ref, weight_send, weight_recv, share_sem, scale_ref, outgoing, hidden,
-        cross_sem, spread_sem, mirror_sem, part_sem, return_sem, home, returned_ref, back_sem,
+        cross_sem, spread_sem, later_sem, mirror_sem, part_sem, return_sem, home, returned_ref, back_sem,
         *per_set,
     ):
         count = len(sets)
@@ -317,6 +317,7 @@
             rows = rotated(
                 q_v[:, pl.ds(head * pair_width, pair_width)].astype(f32), both_gains[0]
             ) * HEAD_DIM ** (-0.5)
+            rows = jnp.dot(perm_ref[...], rows.astype(bf16), preferred_element_type=f32)
             q_pad[head, pl.ds(0, token_count)] = jnp.where(low_half, rows, 0.0).astype(bf16)
             q_pad[head, pl.ds(token_count, token_count)] = jnp.where(
                 low_half, swap(rows), 0.0
@@ -370,11 +371,16 @@
         waiting = []
         for part in range(pieces):
             pass_on(1, part)
+        route()
         for head in range(key_heads):
             prepare(head)
-        route()
         waiting += [(0, head, True) for head in range(key_heads)]
         for hop in range(2, ring_half + 1):
+            if hop == 3:
+                loads[4].wait()
+                res_ref[...] = jnp.dot(
+                    perm_ref[...], res_ref[...], preferred_element_type=f32
+                ).astype(bf16)
             for part in range(pieces):
                 pass_on(hop, part)
                 for _ in range(-(-len(waiting) // (pieces - part))):
@@ -437,7 +443,6 @@
         total = mix(me_t)
         pair[0].wait_recv()
         total = total + mix_pair[0].astype(f32)
-        loads[4].wait()
         total = total + residual_scale * res_ref[...].astype(f32)
         for step in range(1, lines):
             with scope("acrosswait"):
@@ -464,7 +469,7 @@
 
         with scope("norm1"):
             normed = normalize(total, gain_ref[...], 0).astype(bf16)
-        spread_rows = jnp.dot(perm_ref[...], normed, preferred_element_type=f32).astype(bf16)
+        spread_rows = normed
         outgoing[...] = spread_rows
         square = [(turn, step) for turn in range(EXP_GROUP) for step in range(lines)]
         square.sort(key=lambda pair: -(pair[0] + 1) // 2 - min(pair[1], lines - pair[1]))
@@ -506,7 +511,7 @@
                 source = routed[index].at[me_t, rows]
             for turn, step in square:
                 arrivals[index, turn, step] = push(
-                    source, routed[index].at[me_t, rows], 4, spread_sem.at[index, turn, step],
+                    source, routed[index].at[me_t, rows], 4, spread_sem.at[turn, step] if index == 0 else later_sem.at[index],
                     square_device(turn, step),
                 )
             push(
@@ -514,8 +519,12 @@
             )
 
         def mirror(index):
+            if index > 0:
+                size = len(square) * member_rows[index] * width * 2
+                waiter(stretch_of(size), later_sem.at[index]).wait_recv()
             for turn, step in square:
-                arrivals[index, turn, step].wait_recv()
+                if index == 0:
+                    arrivals[index, turn, step].wait_recv()
                 block = routed[index].at[
                     line_before(step) * 2 + core, member_span(index, member(turn))
                 ]
@@ -525,25 +534,21 @@
             size = lines * set_rows[index] * width * 2
             waiter(stretch_of(size), mirror_sem.at[index]).wait_recv()
 
-        def expand(index):
+        def expand(index, span):
             base = sum(set_rows[:index])
             rows = set_rows[index]
 
             def one_tile(number, carry):
                 cols = pl.ds(pl.multiple_of(number * tile, tile), tile)
-                gate_sum = jnp.zeros((rows, tile), f32)
-                up_sum = jnp.zeros((rows, tile), f32)
-                for shard in range(shards):
-                    block = routed[index][shard]
-                    deep = pl.ds(shard * width, width)
-                    gate_sum += jnp.dot(block, gate_v[deep, cols], preferred_element_type=f32)
-                    up_sum += jnp.dot(block, up_v[deep, cols], preferred_element_type=f32)
+                block = jnp.concatenate([routed[index][shard] for shard in range(shards)], 1)
+                gate_sum = jnp.dot(block, gate_v[:, cols], preferred_element_type=f32)
+                up_sum = jnp.dot(block, up_v[:, cols], preferred_element_type=f32)
                 hidden[pl.ds(base, rows), cols] = (
                     gate_sum / (1.0 + jnp.exp(-gate_sum)) * up_sum
                 ).astype(bf16)
                 return carry
 
-            lax.fori_loop(0, hidden_units // tile, one_tile, 0)
+            lax.fori_loop(*span, one_tile, 0)
 
         def down(index, shard):
             base = sum(set_rows[:index])
@@ -622,22 +627,24 @@
         with scope("weights"):
             for load in loads[5:]:
                 load.wait()
+        tiles = hidden_units // tile
         for index in range(len(sets)):
             with scope(f"settle{index}"):
                 settle(index)
-            with scope(f"expand{index}"):
-                expand(index)
+            with scope(f"expand{index}a"):
+                expand(index, (0, min(1, tiles)))
+            if index > 0:
+                with scope(f"join{index - 1}"):
+                    join(index - 1)
+            with scope(f"expand{index}b"):
+                expand(index, (min(1, tiles), tiles))
             if index + 1 < len(sets):
                 with scope(f"mirror{index + 1}"):
                     mirror(index + 1)
-            if index == 1:
-                with scope("join0"):
-                    join(0)
             with scope(f"shrink{index}"):
                 shrink(index)
-            if index > 0 or len(sets) == 1:
-                with scope(f"join{index}"):
-                    join(index)
+        with scope("join_last"):
+            join(len(sets) - 1)
         backs = {}
         for order, index in enumerate(away_sets):
             with scope(f"gather{index}"):
@@ -724,7 +731,8 @@
             pltpu.VMEM((token_count, width), bf16),
             pltpu.VMEM((row_total, hidden_units), bf16),
             dma((splits, max(groups - 1, 1))),
-            dma((len(sets), EXP_GROUP, lines)),
+            dma((EXP_GROUP, lines)),
+            dma((len(sets),)),
             dma((len(sets),)),
             dma((len(sets), lines)),
             dma((len(sets),)),

time: 64.5 us -> 63.4 us (0.983)
  Pallas kernels: 63.6 us -> 62.5 us
    pallas_call x1, Pallas kernels: 63.6 us -> 62.5 us  [layer(): pl.pallas_call(kernel, out_shape=pltpu.VMEM((token_count, width), bf16),...]
where the time goes in v5:
time: 63.4 us; the launch traced here: 63.1 us
  Pallas kernels  62.5 us (99%)
  local copies, waits for them, and re-layouts  0.66 us (1%)
    pallas_call x1, Pallas kernels, layer(): pl.pallas_call(kernel, out_shape=pltpu.VMEM((token_count, width), bf16),...  62.5 us

profile of v5, /device:TPU:0, one launch (start us, length us, event | category | flops | bytes accessed | tf_op | source)
XLA Modules:
  0.0 63.1 jit_solution(4953263823971753650)
XLA Ops:
  0.0 62.5 %shard_map.154 = bf16[128,512]{1,0:T(8,128)(2,1)S(1)} custom-call(f32[2,16,128]{2,1,0:T(8,128)} %constant.4.clone.row_hbm, f32[2,64,128]{2,1,0:T(8,128)} %constant.5.clone.column_hbm, f32[1,64]{1,0:T(1,128)} %bitcast.10, f32[1,64]{1,0:T(1,128)} %bitcast.11, f32[1,512]{1,0:T(1,128)} %bitcast.6, s32[2,128]{1,0:T(2,128)} %bitcast.8, f32[2,128]{1,0:T(2,128)} %bitcast.9, ...), custom_call_target="tpu_custom_call" | custom-call | tf_op jit(solution)/shard_map/pallas_call | solution.py:684
  62.5 0.7 %copy.18 = bf16[128,512]{1,0:T(8,128)(2,1)} copy(bf16[128,512]{1,0:T(8,128)(2,1)S(1)} %shard_map.154) | data formatting | bytes 262144

commit v6 on v5

--- a/solution.py
+++ b/solution.py
@@ -97,7 +97,7 @@
     set_rows = [EXP_GROUP * rows for rows in member_rows]
     row_total = sum(set_rows)
     hidden_units = gate_weight.shape[2]
-    tile = min(256, hidden_units)
+    tile = min(512, hidden_units)
     feature_total = width * shards
     bf16, f32 = jnp.bfloat16, jnp.float32
 

time: 63.4 us -> 62.3 us (0.983)
  Pallas kernels: 62.5 us -> 61.4 us
    pallas_call x1, Pallas kernels: 62.5 us -> 61.4 us  [layer(): pl.pallas_call(kernel, out_shape=pltpu.VMEM((token_count, width), bf16),...]
where the time goes in v6:
time: 62.3 us; the launch traced here: 62.1 us
  Pallas kernels  61.4 us (99%)
  local copies, waits for them, and re-layouts  0.66 us (1%)
    pallas_call x1, Pallas kernels, layer(): pl.pallas_call(kernel, out_shape=pltpu.VMEM((token_count, width), bf16),...  61.4 us

profile of v6, /device:TPU:0, one launch (start us, length us, event | category | flops | bytes accessed | tf_op | source)
XLA Modules:
  0.0 62.1 jit_solution(17251923052707279153)
XLA Ops:
  0.0 61.4 %shard_map.154 = bf16[128,512]{1,0:T(8,128)(2,1)S(1)} custom-call(f32[2,16,128]{2,1,0:T(8,128)} %constant.4.clone.row_hbm, f32[2,64,128]{2,1,0:T(8,128)} %constant.5.clone.column_hbm, f32[1,64]{1,0:T(1,128)} %bitcast.10, f32[1,64]{1,0:T(1,128)} %bitcast.11, f32[1,512]{1,0:T(1,128)} %bitcast.6, s32[2,128]{1,0:T(2,128)} %bitcast.8, f32[2,128]{1,0:T(2,128)} %bitcast.9, ...), custom_call_target="tpu_custom_call" | custom-call | tf_op jit(solution)/shard_map/pallas_call | solution.py:684
  61.4 0.7 %copy.18 = bf16[128,512]{1,0:T(8,128)(2,1)} copy(bf16[128,512]{1,0:T(8,128)(2,1)S(1)} %shard_map.154) | data formatting | bytes 262144
